TPU v7x, 32 devices: a whole 2x2x4 slice. The times are simulated.
32 devices in a mesh: sp: 4 (over z), fs: 4 (over y, x), tp: 2 (over core).
Axes of the slice: x: 2, y: 2, z: 4, core: 2. Of those that a mesh axis runs over, the one named last changes fastest.
Arguments:
- inputs: bfloat16 [2048, 2048], P(('fs', 'sp'), 'tp'), parts along dimension 0, may hold values from -6 to 6
- norm_gain: float32 [2048], replicated, may hold values from 0.1 to 1.9
- in_ssm: bfloat16 [2048, 1024], P('sp', 'tp'), may hold values from -0.125 to 0.125
- in_query: bfloat16 [2048, 1024], P('sp', 'tp')
- in_key: bfloat16 [2048, 256], P('sp', 'tp')
- in_value: bfloat16 [2048, 256], P('sp', 'tp'), may hold values from -0.125 to 0.125
- decay_rate: float32 [64, 64], P('tp'), as said below
- rotation: float32 [64, 64], P('tp'), may hold values from 0.05 to 3
- input_parts: bfloat16 [2, 64, 64, 16], P(None, 'tp')
- output_parts: bfloat16 [2, 64, 16, 64], P(None, 'tp'), may hold values from -0.5 to 0.5
- skip_scale: float32 [64, 16], P('tp'), may hold values from -4 to 4
- decay_shift: float32 [2048, 64], P(('fs', 'sp'), 'tp'), parts along dimension 0, may hold values from -1 to 0
- sink_logit: float32 [16], P('tp'), may hold values from 2 to 6
- out_state: bfloat16 [1024, 2048], P('tp', 'sp'), may hold values from -0.125 to 0.125
- out_attend: bfloat16 [1024, 2048], P('tp', 'sp'), may hold values from -0.125 to 0.125
Outputs:
- mixed: bfloat16 [2048, 2048], P(('fs', 'sp', 'tp')), parts along dimension 0
There are 4 independent parts, one for each index of `fs`. A program takes and returns all parts, laid end to end along the dimension named above; an argument that names none is the same for every part. Nothing has to cross between parts.
Inputs may be any that keep to these rules, and one draw needn't show every extreme that they name: `decay_rate`: between 1e-5 and 0.1.
All inputs are finite; a program needn't handle non-finite values.
Results may differ from a plain program's by a relative error of at most 0.012.
Values may be sent and summed in bfloat16 or wider, within the bound.
A program may use at most 64 MiB of HBM per device.

v0:
```python
import jax
import jax.numpy as jnp
from jax import lax
from jax.sharding import PartitionSpec as P

GROUP_CH = 16
HEAD_DIM = 64
WINDOW = 128
BLOCK = 128


epsilon = 1e-06
floor_score = -1e30


def prefix(x, axis, join, neutral):
    place = lax.axis_index(axis)
    gathered = jax.tree.map(
        lambda a, kind: lax.all_gather(a.astype(kind), axis),
        x,
        (jnp.bfloat16, jnp.bfloat16, jnp.bfloat16, jnp.bfloat16),
    )
    state = jax.tree.map(lambda a, e: jnp.zeros_like(a) + jnp.asarray(e, a.dtype), x, neutral)

    def one(hop, state):
        return join(
            state,
            jax.tree.map(
                lambda a, own: lax.dynamic_index_in_dim(a, hop, 0, False).astype(own.dtype),
                gathered,
                x,
            ),
        )

    return lax.fori_loop(0, place, one, state)


def from_behind(value, axis, steps):
    count = lax.axis_size(axis)
    initial, last = (max(0, -steps), min(count, count - steps))
    return lax.ppermute(value, axis, [(source, source + steps) for source in range(initial, last)])


def combine(earlier, later):
    first_re, first_im, state_re, state_im = earlier
    second_re, second_im, input_re, input_im = later
    return (
        second_re * first_re - second_im * first_im,
        second_re * first_im + second_im * first_re,
        second_re * state_re - second_im * state_im + input_re,
        second_re * state_im + second_im * state_re + input_im,
    )


def input_matrix(decay_rate, rotation, input_parts):
    damped = jnp.exp(-decay_rate)
    lift_re = damped * jnp.cos(rotation) - 1.0
    lift_im = damped * jnp.sin(rotation)
    modulus = decay_rate * decay_rate + rotation * rotation
    factor_re = (rotation * lift_im - decay_rate * lift_re) / modulus
    factor_im = -(rotation * lift_re + decay_rate * lift_im) / modulus
    part_re = input_parts[0].astype(jnp.float32)
    part_im = input_parts[1].astype(jnp.float32)
    joined_re = factor_re[:, :, None] * part_re - factor_im[:, :, None] * part_im
    joined_im = factor_re[:, :, None] * part_im + factor_im[:, :, None] * part_re
    return jnp.concatenate([joined_re, joined_im], axis=1).astype(jnp.bfloat16)


def window_attention(queries, keys_win, values_win, starts, sink_logit):
    window = queries.shape[1]
    scores = jnp.einsum("nqgrd,nkgd->ngrqk", queries, keys_win, preferred_element_type=jnp.float32)
    scores = scores * queries.shape[-1] ** (-0.5)
    places = (
        jnp.arange(window, dtype=jnp.int32)[:, None]
        + window
        - jnp.arange(2 * window, dtype=jnp.int32)[None, :]
    )
    inside = (places >= 0) & (places < window)
    reach = starts[:, None] - window + jnp.arange(2 * window, dtype=jnp.int32)[None, :] >= 0
    valid = (inside[None] & reach[:, None, :])[:, None, None]
    sinks = sink_logit.reshape(scores.shape[1], scores.shape[2])[None, :, :, None, None]
    scores = jnp.where(valid, scores, floor_score)
    row_peak = jnp.maximum(jnp.max(scores, axis=-1, keepdims=True), sinks)
    raised = jnp.where(valid, jnp.exp(scores - row_peak), 0.0)
    denominator = jnp.sum(raised, axis=-1, keepdims=True) + jnp.exp(sinks - row_peak)
    weights = (raised / denominator).astype(jnp.bfloat16)
    result = jnp.einsum(
        "ngrqk,nkgd->nqgrd", weights, values_win, preferred_element_type=jnp.float32
    )
    return result.astype(jnp.bfloat16)


def body(
    inputs,
    norm_gain,
    in_ssm,
    in_query,
    in_key,
    in_value,
    decay_rate,
    rotation,
    input_parts,
    output_parts,
    skip_scale,
    decay_shift,
    sink_logit,
    out_state,
    out_attend,
):
    gathered = lax.all_gather(inputs, "tp", axis=1, tiled=True)
    length = gathered.shape[0]
    widened = gathered.astype(jnp.float32)
    scale = lax.rsqrt(jnp.mean(widened * widened, axis=1, keepdims=True) + epsilon)
    normed = (widened * scale * norm_gain).astype(jnp.bfloat16)

    def add_rows(pieces):
        return tuple(
            (jnp.dot(normed, piece, preferred_element_type=jnp.float32) for piece in pieces)
        )

    projected = add_rows(
        (
            lax.all_gather(in_ssm, "sp", axis=0, tiled=True),
            lax.all_gather(in_query, "sp", axis=0, tiled=True),
            lax.all_gather(in_key, "sp", axis=0, tiled=True),
            lax.all_gather(in_value, "sp", axis=0, tiled=True),
        )
    )
    drive_in, queries, keys_local, values = [piece.astype(jnp.bfloat16) for piece in projected]
    groups = decay_rate.shape[0]
    state_dim = decay_rate.shape[1]
    channels = groups * GROUP_CH
    highest = lax.Precision.HIGHEST
    drive_cols = jnp.transpose(drive_in).reshape(groups, GROUP_CH, length)
    in_matrix = input_matrix(decay_rate, rotation, input_parts)
    drive = jnp.einsum("gqh,ght->gqt", in_matrix, drive_cols, preferred_element_type=jnp.float32)
    shift_cols = jnp.transpose(decay_shift)
    running = jnp.cumsum(shift_cols, axis=1)
    total_shift = running[:, -1]
    remain = length - 1.0 - jnp.arange(length, dtype=jnp.float32)
    to_end = (total_shift[:, None] - running)[:, None, :] - decay_rate[:, :, None] * remain[
        None, None, :
    ]
    fade = jnp.exp(to_end)
    turn = rotation[:, :, None] * remain[None, None, :]
    weight_re = fade * jnp.cos(turn)
    weight_im = fade * jnp.sin(turn)
    drive_re = drive[:, :state_dim]
    drive_im = drive[:, state_dim:]
    final_re = jnp.sum(weight_re * drive_re - weight_im * drive_im, axis=2)
    final_im = jnp.sum(weight_re * drive_im + weight_im * drive_re, axis=2)
    overall = jnp.exp(total_shift[:, None] - decay_rate * length)
    nothing = jnp.zeros_like(final_re)
    carried = prefix(
        (
            overall * jnp.cos(rotation * length),
            overall * jnp.sin(rotation * length),
            final_re,
            final_im,
        ),
        "sp",
        combine,
        (jnp.ones_like(final_re), nothing, nothing, nothing),
    )
    key_heads = keys_local.shape[1] // HEAD_DIM
    query_heads = queries.shape[1] // HEAD_DIM
    windows_dev = length // WINDOW
    previous = from_behind((keys_local, values), "sp", 1)

    def windows(flat, before):
        split = jnp.concatenate([before, flat], axis=0).reshape(
            windows_dev + 1, WINDOW, key_heads, HEAD_DIM
        )
        return jnp.concatenate([split[:-1], split[1:]], axis=1)

    offset = lax.axis_index("sp") * length
    starts = offset + jnp.arange(windows_dev, dtype=jnp.int32) * WINDOW
    queries_blk = queries.reshape(
        windows_dev, WINDOW, key_heads, query_heads // key_heads, HEAD_DIM
    )
    attended = window_attention(
        queries_blk,
        windows(keys_local, previous[0]),
        windows(values, previous[1]),
        starts,
        sink_logit,
    )
    attend_out = attended.reshape(length, query_heads * HEAD_DIM)
    blocks = length // BLOCK
    triangle = (
        jnp.arange(BLOCK, dtype=jnp.int32)[:, None] <= jnp.arange(BLOCK, dtype=jnp.int32)[None, :]
    ).astype(jnp.float32)
    offsets = jnp.arange(BLOCK, dtype=jnp.float32)
    centre = BLOCK // 2
    read_re = output_parts[0].astype(jnp.float32)
    read_im = output_parts[1].astype(jnp.float32)
    angle = rotation[:, :, None] * (offsets - centre)[None, None, :]
    cos_angle = jnp.cos(angle)
    sin_angle = jnp.sin(angle)
    phase = rotation[:, :, None] * (offsets + 1.0)[None, None, :]
    cos_phase = jnp.cos(phase)
    sin_phase = jnp.sin(phase)

    def advance(carry, pieces):
        carry_re, carry_im = carry
        part_re, part_im, shift_part, grouped_part = pieces
        level = jnp.dot(shift_part, triangle, precision=highest)
        log_from = level[:, None, :] - decay_rate[:, :, None] * (offsets + 1.0)[None, None, :]
        relative = log_from - log_from[:, :, centre : centre + 1]
        shrink = jnp.exp(-relative)
        lift_re = shrink * (part_re * cos_angle + part_im * sin_angle)
        lift_im = shrink * (part_im * cos_angle - part_re * sin_angle)
        prefix_re = jnp.dot(lift_re.reshape(groups * state_dim, BLOCK), triangle, precision=highest)
        prefix_im = jnp.dot(lift_im.reshape(groups * state_dim, BLOCK), triangle, precision=highest)
        prefix_re = prefix_re.reshape(groups, state_dim, BLOCK)
        prefix_im = prefix_im.reshape(groups, state_dim, BLOCK)
        grow = jnp.exp(relative)
        from_start = jnp.exp(log_from)
        keep_re = from_start * cos_phase
        keep_im = from_start * sin_phase
        state_re = grow * (prefix_re * cos_angle - prefix_im * sin_angle)
        state_im = grow * (prefix_im * cos_angle + prefix_re * sin_angle)
        state_re = state_re + keep_re * carry_re[:, :, None] - keep_im * carry_im[:, :, None]
        state_im = state_im + keep_re * carry_im[:, :, None] + keep_im * carry_re[:, :, None]
        result = jnp.einsum("ghp,gpt->ght", read_re, state_re, precision=highest)
        result = result - jnp.einsum("ghp,gpt->ght", read_im, state_im, precision=highest)
        result = result + skip_scale[:, :, None] * grouped_part.astype(jnp.float32)
        return ((state_re[:, :, -1], state_im[:, :, -1]), jax.nn.gelu(result).astype(jnp.bfloat16))

    drive_blocks = jnp.transpose(drive.reshape(groups, 2 * state_dim, blocks, BLOCK), (2, 0, 1, 3))
    shift_blocks = jnp.transpose(shift_cols.reshape(groups, blocks, BLOCK), (1, 0, 2))
    grouped_blocks = jnp.transpose(
        drive_cols.reshape(groups, GROUP_CH, blocks, BLOCK), (2, 0, 1, 3)
    )
    _, state_blocks = lax.scan(
        advance,
        (carried[2], carried[3]),
        (
            drive_blocks[:, :, :state_dim],
            drive_blocks[:, :, state_dim:],
            shift_blocks,
            grouped_blocks,
        ),
    )
    state_out = jnp.transpose(state_blocks, (0, 3, 1, 2)).reshape(length, channels)
    column_state, column_attend = (
        lax.all_gather(out_state, "sp", axis=1, tiled=True),
        lax.all_gather(out_attend, "sp", axis=1, tiled=True),
    )
    result = jnp.dot(state_out, column_state, preferred_element_type=jnp.float32)
    return lax.psum_scatter(
        (result + jnp.dot(attend_out, column_attend, preferred_element_type=jnp.float32)).astype(
            jnp.bfloat16
        ),
        "tp",
        scatter_dimension=0,
        tiled=True,
    )


def solution(mesh):
    return jax.shard_map(
        body,
        mesh=mesh,
        in_specs=(
            P(("fs", "sp"), "tp"),
            P(),
            P("sp", "tp"),
            P("sp", "tp"),
            P("sp", "tp"),
            P("sp", "tp"),
            P("tp", None),
            P("tp", None),
            P(None, "tp", None, None),
            P(None, "tp", None, None),
            P("tp", None),
            P(("fs", "sp"), "tp"),
            P("tp"),
            P("tp", "sp"),
            P("tp", "sp"),
        ),
        out_specs=P(("fs", "sp", "tp"), None),
        check_vma=False,
    )
```

profile of v0, /device:TPU:0, one launch (start us, length us, event | category | flops | bytes accessed | tf_op | source)
XLA Modules:
  0.0 228.4 jit_solution(4476878250785179290)
XLA Ops:
  6.5 0.7 all-gather.13.cloned.1.call-update
  7.3 0.0 all-gather.9.cloned.1.call-start
  7.3 0.7 all-gather.9.cloned.1.call-update
  8.1 0.7 all-gather.11.cloned.1.call-update
  8.8 2.5 %all_gather.41 = bf16[128,2048]{1,0:T(8,128)(2,1)S(1)} all-gather(bf16[128,1024]{1,0:T(8,128)(2,1)} %param.17), channel_id=1, replica_groups=mesh['sp'=4,'fs'=4,'tp'=2] {'tp'}, dimensions={1}, use_global_device_ids=true | all-gather | bytes 786432 | tf_op jit(solution)/shard_map/all_gather | solution.py:110
  11.3 0.2 fusion.18
  11.6 23.0 %all_gather.51 = bf16[2048,128]{1,0:T(8,128)(2,1)S(1)} all-gather(bf16[512,128]{1,0:T(8,128)(2,1)S(1)} %copy-done.1), channel_id=1, replica_groups=mesh['sp'=4,'fs'=4,'tp'=2] {'sp'}, dimensions={0}, use_global_device_ids=true | all-gather | bytes 655360 | tf_op jit(solution)/shard_map/all_gather | solution.py:125
  34.6 0.4 convolution_convert_fusion.3
  35.0 2.2 collective-permute-start.1
  37.2 22.5 %all_gather.50 = bf16[2048,128]{1,0:T(8,128)(2,1)S(1)} all-gather(bf16[512,128]{1,0:T(8,128)(2,1)S(1)} %copy-done.2), channel_id=1, replica_groups=mesh['sp'=4,'fs'=4,'tp'=2] {'sp'}, dimensions={0}, use_global_device_ids=true | all-gather | bytes 655360 | tf_op jit(solution)/shard_map/all_gather | solution.py:126
  59.7 0.4 convolution_convert_fusion.4
  60.1 1.7 collective-permute-start
  61.9 0.0 reduce-scatter.2.cloned.1.call-start
  62.0 0.1 max.18
  62.1 0.1 convolution_bitcast_fusion
  62.2 0.3 reduce_window_sum.11
  62.5 0.2 slice_reduce_fusion.1
  62.7 0.1 broadcast_subtract_fusion
  62.8 0.2 multiply_convert_fusion
  63.0 13.3 %all-gather = bf16[128,64]{1,0:T(8,128)(2,1)S(1)} all-gather(bf16[32,64]{1,0:T(8,128)(2,1)S(1)} %get-tuple-element.154), channel_id=2, replica_groups=mesh['sp'=4,'fs'=4,'tp'=2] {'sp'}, dimensions={0}, use_global_device_ids=true | all-gather | bytes 20480 | tf_op jit(solution)/shard_map/all_gather | solution.py:19
  76.2 13.6 %all-gather.1 = bf16[128,64]{1,0:T(8,128)(2,1)S(1)} all-gather(bf16[32,64]{1,0:T(8,128)(2,1)S(1)} %get-tuple-element.153), channel_id=3, replica_groups=mesh['sp'=4,'fs'=4,'tp'=2] {'sp'}, dimensions={0}, use_global_device_ids=true | all-gather | bytes 20480 | tf_op jit(solution)/shard_map/all_gather | solution.py:19
  89.9 0.1 copy.22
  89.9 0.1 fusion.117
  90.0 0.1 fusion.91
  90.2 2.1 convolution_convert_fusion.1
  92.3 0.1 copy.23
  92.4 0.4 fusion.134
  92.8 0.1 broadcast_maximum_fusion
  92.8 0.2 fusion.60
  93.0 0.1 exponential_add_fusion
  93.1 26.0 %all-gather.9.cloned.1.call-done = bf16[2048,512]{1,0:T(8,128)(2,1)} async-done(((bf16[512,512]{1,0:T(8,128)(2,1)}), bf16[2048,512]{1,0:T(8,128)(2,1)}) %all-gather.9.cloned.1.call-update) | async-done | bytes 2097168 | tf_op jit(solution)/shard_map/all_gather | solution.py:123
  119.1 2.1 fusion.17
  121.2 0.1 copy.21
  121.3 0.9 fusion.106
  122.2 5.1 %add_reduce_fusion = (bf16[32,64]{1,0:T(8,128)(2,1)S(1)}, bf16[32,64]{1,0:T(8,128)(2,1)S(1)}, f32[32,64,128]{2,1,0:T(8,128)S(1)}) fusion(f32[32,128,128]{2,1,0:T(8,128)S(1)} %fusion.106, f32[128]{0:T(128)S(1)} %get-tuple-element.160, f32[32,128]{1,0:T(8,128)S(1)} %broadcast_subtract_fusion, f32[32,64]{1,0:T(8,128)S(1)} %copy-done.3, ...), kind=kLoop, calls=%fused_computation.70 | loop fusion | flops 3928064 | bytes 3204096 | tf_op jit(solution)/shard_map/reduce_sum | solution.py:151
  127.3 0.6 slice_reduce_fusion
  128.0 13.7 %all-gather.2 = bf16[128,64]{1,0:T(8,128)(2,1)S(1)} all-gather(bf16[32,64]{1,0:T(8,128)(2,1)S(1)} %get-tuple-element.132), channel_id=4, replica_groups=mesh['sp'=4,'fs'=4,'tp'=2] {'sp'}, dimensions={0}, use_global_device_ids=true | all-gather | bytes 20480 | tf_op jit(solution)/shard_map/all_gather | solution.py:19
  141.7 14.0 %all-gather.3 = bf16[128,64]{1,0:T(8,128)(2,1)S(1)} all-gather(bf16[32,64]{1,0:T(8,128)(2,1)S(1)} %get-tuple-element.131), channel_id=5, replica_groups=mesh['sp'=4,'fs'=4,'tp'=2] {'sp'}, dimensions={0}, use_global_device_ids=true | all-gather | bytes 20480 | tf_op jit(solution)/shard_map/all_gather | solution.py:19
  155.7 0.4 convolution_convert_fusion
  156.1 4.7 %fusion.23 = f32[32,64,128]{2,1,0:T(8,128)S(1)} fusion(f32[1,32,128,128]{3,2,1,0:T(8,128)S(1)} %bitcast.122, f32[128]{0:T(128)S(1)} %iota_add_fusion.1, f32[32,64]{1,0:T(8,128)S(1)} %copy-done.3, f32[32,64]{1,0:T(8,128)S(1)} %slice_reduce_fusion, f32[128]{0:T(128)S(1)} %get-tuple-element.161, f32[32,64]{1,0:T(8,128)S(1)} %copy-done.4, ...), kind=kOutput, calls=%fused_computation.44 | convolution fusion | flops 405028864 | bytes 3187712 | tf_op jit(solution)/shard_map/while/body/eval_jaxpr/dot_general | solution.py:213
  160.8 4.7 %fusion.27 = f32[32,64,128]{2,1,0:T(8,128)S(1)} fusion(f32[1,32,128,128]{3,2,1,0:T(8,128)S(1)} %bitcast.123, f32[128]{0:T(128)S(1)} %iota_add_fusion.1, f32[32,64]{1,0:T(8,128)S(1)} %copy-done.3, f32[32,64]{1,0:T(8,128)S(1)} %slice_reduce_fusion, f32[128]{0:T(128)S(1)} %get-tuple-element.161, f32[32,64]{1,0:T(8,128)S(1)} %copy-done.4, ...), kind=kOutput, calls=%fused_computation.47 | convolution fusion | flops 405028864 | bytes 3187712 | tf_op jit(solution)/shard_map/while/body/eval_jaxpr/dot_general | solution.py:214
  165.5 0.2 while.3
  165.7 8.6 %fusion.33 = f32[32,128,16]{1,2,0:T(8,128)S(1)} fusion(f32[32,64,128]{2,1,0:T(8,128)S(1)} %fusion.27, f32[32,64,128]{2,1,0:T(8,128)S(1)} %fusion.23, f32[32,64]{1,0:T(8,128)S(1)} %get-tuple-element.130, f32[32,64]{1,0:T(8,128)S(1)} %get-tuple-element.129, f32[128]{0:T(128)S(1)} %iota_add_fusion.1, f32[32,64]{1,0:T(8,128)S(1)} %copy-done.3, ...), kind=kOutput, calls=%fused_computation.52 | convolution fusion | flops 54263808 | bytes 2589696 | tf_op jit(solution)/shard_map/while/body/eval_jaxpr/ghp,gpt->ght/dot_general | solution.py:225
  174.3 10.4 %fusion.103 = bf16[32,16,128]{2,1,0:T(8,128)(2,1)S(1)} fusion(f32[32,128,16]{1,2,0:T(8,128)S(1)} %fusion.33, f32[32,64,128]{2,1,0:T(8,128)S(1)} %fusion.23, f32[32,64,128]{2,1,0:T(8,128)S(1)} %fusion.27, f32[32,64]{1,0:T(8,128)S(1)} %get-tuple-element.130, f32[32,64]{1,0:T(8,128)S(1)} %get-tuple-element.129, f32[128]{0:T(128)S(1)} %iota_add_fusion.1, ...), kind=kOutput, calls=%fused_computation.123 | convolution fusion | flops 55115776 | bytes 2868224 | tf_op jit(solution)/shard_map/while/body/eval_jaxpr/ghp,gpt->ght/dot_general | solution.py:226
  184.7 2.1 fusion.135
  186.8 25.3 %all-gather.15.cloned.1.call-done = bf16[512,2048]{1,0:T(8,128)(2,1)} async-done(((bf16[512,512]{1,0:T(8,128)(2,1)}), bf16[512,2048]{1,0:T(8,128)(2,1)}) %all-gather.15.cloned.1.call-update) | async-done | bytes 2097168 | tf_op jit(solution)/shard_map/all_gather | solution.py:248
  212.1 2.9 %fusion.4 = bf16[128,2048]{1,0:T(8,128)(2,1)} fusion(f32[128,2048]{1,0:T(8,128)S(1)} %fusion.135, bf16[128,512]{0,1:T(8,128)(2,1)S(1)} %bitcast.132, bf16[512,2048]{1,0:T(8,128)(2,1)} %all-gather.15.cloned.1.call-done), kind=kOutput, calls=%fused_computation.9 | convolution fusion | flops 268959744 | bytes 3801088 | tf_op jit(solution)/shard_map/dot_general | solution.py:252
  215.0 6.9 %reduce-scatter.2.cloned.1.call-done = bf16[64,2048]{1,0:T(8,128)(2,1)} async-done(((bf16[128,2048]{1,0:T(8,128)(2,1)}), bf16[64,2048]{1,0:T(8,128)(2,1)}) %reduce-scatter.2.cloned.1.call-update) | async-done | bytes 262160 | tf_op jit(solution)/shard_map/reduce_scatter | solution.py:251
  (36 shorter events, 0.2 us)
Async XLA Ops:
  6.5 5.0 %copy-start.1 = (bf16[512,128]{1,0:T(8,128)(2,1)S(1)}, bf16[512,128]{1,0:T(8,128)(2,1)}, u32[]{:S(2)}) copy-start(bf16[512,128]{1,0:T(8,128)(2,1)} %param.21) | copy-start | bytes 393220
  6.5 28.0 %copy-start.8 = (f32[2048]{0:T(1024)S(1)}, f32[2048]{0:T(1024)}, u32[]{:S(2)}) copy-start(f32[2048]{0:T(1024)} %param.18) | copy-start | bytes 24580
  6.5 83.6 %all-gather.13.cloned.1.call-start = ((), (), s32[]{:S(2)}) async-start(), calls=%async_computation.3 | async-start | bytes 2621440 | tf_op jit(solution)/shard_map/all_gather | solution.py:124
  7.3 29.9 %copy-start.2 = (bf16[512,128]{1,0:T(8,128)(2,1)S(1)}, bf16[512,128]{1,0:T(8,128)(2,1)}, u32[]{:S(2)}) copy-start(bf16[512,128]{1,0:T(8,128)(2,1)} %param.22) | copy-start | bytes 393220
  7.3 111.9 %all-gather.9.cloned.1.call-start = ((), (), s32[]{:S(2)}) async-start(), calls=%async_computation.1 | async-start | bytes 2621440 | tf_op jit(solution)/shard_map/all_gather | solution.py:123
  8.0 176.7 %all-gather.11.cloned.1.call-start = ((), (), s32[]{:S(2)}) async-start(), calls=%async_computation.2 | async-start | bytes 2621440 | tf_op jit(solution)/shard_map/all_gather | solution.py:247
  8.8 203.4 %all-gather.15.cloned.1.call-start = ((), (), s32[]{:S(2)}) async-start(), calls=%async_computation.4 | async-start | bytes 2621440 | tf_op jit(solution)/shard_map/all_gather | solution.py:248
  11.5 50.5 %copy-start.9 = (f32[8]{0:T(128)S(1)}, f32[8]{0:T(128)}, u32[]{:S(2)}) copy-start(f32[8]{0:T(128)} %param.29) | copy-start | bytes 100
  11.5 50.6 %copy-start.5 = (f32[128,32]{0,1:T(8,128)S(1)}, f32[128,32]{0,1:T(8,128)}, u32[]{:S(2)}) copy-start(f32[128,32]{0,1:T(8,128)} %param.28) | copy-start | bytes 49156
  11.5 51.3 %copy-start.3 = (f32[32,64]{1,0:T(8,128)S(1)}, f32[32,64]{1,0:T(8,128)}, u32[]{:S(2)}) copy-start(f32[32,64]{1,0:T(8,128)} %param.24) | copy-start | bytes 24580
  11.5 51.3 %copy-start.4 = (f32[32,64]{1,0:T(8,128)S(1)}, f32[32,64]{1,0:T(8,128)}, u32[]{:S(2)}) copy-start(f32[32,64]{1,0:T(8,128)} %param.23) | copy-start | bytes 24580
  34.5 55.3 %copy-start.6 = (f32[32,16]{0,1:T(8,128)S(1)}, f32[32,16]{0,1:T(8,128)}, u32[]{:S(2)}) copy-start(f32[32,16]{0,1:T(8,128)} %param.27) | copy-start | bytes 6148
  34.5 55.5 %copy-start = (bf16[2,32,64,16]{2,3,1,0:T(8,128)(2,1)S(1)}, bf16[2,32,64,16]{2,3,1,0:T(8,128)(2,1)}, u32[]{:S(2)}) copy-start(bf16[2,32,64,16]{2,3,1,0:T(8,128)(2,1)} %param.25) | copy-start | bytes 393220
  35.0 57.4 %collective-permute-start.1 = (bf16[128,128]{0,1:T(8,128)(2,1)S(1)}, bf16[128,128]{0,1:T(8,128)(2,1)S(1)}, u32[]{:S(2)}, u32[]{:S(2)}) collective-permute-start(bf16[128,128]{0,1:T(8,128)(2,1)S(1)} %convolution_convert_fusion.3), channel_id=1, source_target_pairs={{0,8},{8,16},{16,24},{1,9},{9,17},{17,25},{2,10},{10,18},{18,26},{... | collective-permute-start | bytes 98312 | tf_op jit(solution)/shard_map/ppermute | solution.py:41
  60.1 95.6 %collective-permute-start = (bf16[128,128]{0,1:T(8,128)(2,1)S(1)}, bf16[128,128]{0,1:T(8,128)(2,1)S(1)}, u32[]{:S(2)}, u32[]{:S(2)}) collective-permute-start(bf16[128,128]{0,1:T(8,128)(2,1)S(1)} %convolution_convert_fusion.4), channel_id=1, source_target_pairs={{0,8},{8,16},{16,24},{1,9},{9,17},{17,25},{2,10},{10,18},{18,26},{... | collective-permute-start | bytes 98312 | tf_op jit(solution)/shard_map/ppermute | solution.py:41
  61.9 160.0 %reduce-scatter.2.cloned.1.call-start = ((), (), s32[]{:S(2)}) async-start(), calls=%async_computation.5 | async-start | bytes 786432 | tf_op jit(solution)/shard_map/reduce_scatter | solution.py:251
  160.8 4.9 %copy-start.7 = (bf16[2,32,16,64]{3,2,1,0:T(8,128)(2,1)S(1)}, bf16[2,32,16,64]{3,2,1,0:T(8,128)(2,1)}, u32[]{:S(2)}) copy-start(bf16[2,32,16,64]{3,2,1,0:T(8,128)(2,1)} %param.26) | copy-start | bytes 393220
Sparse Core Ops, SparseCore 0:
  8.9 61.1 all-gather.12
  71.6 47.4 all-gather.8
  120.7 45.4 all-gather.10
  167.6 44.4 all-gather.14
  215.1 6.7 reduce-scatter.1
where the time goes:
time: 229 us; the launch traced here: 228 us
  blocking collectives  103 us (45%)
  waiting for transfers between devices  60.3 us (26%)
  matrix products  40 us (17%)
  between operations  13.4 us (6%)
  other arithmetic  6.39 us (3%)
  starting transfers between devices  4.06 us (2%)
    all_gather x4, blocking collectives, prefix(): lax.all_gather(a.astype(kind), axis)  54.7 us
    all_gather x1, waiting for transfers between devices, body(): lax.all_gather(in_ssm, 'sp', axis=0, tiled=True)  26 us
    all_gather x1, waiting for transfers between devices, body(): lax.all_gather(out_attend, 'sp', axis=1, tiled=True)  25.3 us
    all_gather x1, blocking collectives, body(): lax.all_gather(in_key, 'sp', axis=0, tiled=True)  23 us
    all_gather x1, blocking collectives, body(): lax.all_gather(in_value, 'sp', axis=0, tiled=True)  22.5 us
    dot_general x1, matrix products, advance(): jnp.einsum('ghp,gpt->ght', read_im, state_im, precision=highest)  10.4 us
    dot_general x1, matrix products, advance(): result = jnp.einsum('ghp,gpt->ght', read_re, state_re, precision=highest)  8.65 us
    reduce_scatter x1, waiting for transfers between devices, body(): lax.psum_scatter((result + jnp.dot(attend_out, column_attend, preferred_e...  6.88 us
  transfers between devices with their start and end apart: 7, of which 3 were waited for; matrix products, arithmetic and copies ran while one was open for 20% of the time, Pallas kernels for 0%

commit v1 on v0

--- a/solution.py
+++ b/solution.py
@@ -1,6 +1,9 @@
+import functools
 import jax
 import jax.numpy as jnp
 from jax import lax
+from jax.experimental import pallas as pl
+from jax.experimental.pallas import tpu as pltpu
 from jax.sharding import PartitionSpec as P
 
 GROUP_CH = 16
@@ -90,7 +93,7 @@
     return result.astype(jnp.bfloat16)
 
 
-def body(
+def general_body(
     inputs,
     norm_gain,
     in_ssm,
@@ -258,6 +261,379 @@
     )
 
 
+MESH = pl.DeviceIdType.MESH
+ANY = pl.BlockSpec(memory_space=pl.ANY)
+
+
+def remote(src, dst, send, recv, **where):
+    return pltpu.make_async_remote_copy(
+        src_ref=src, dst_ref=dst, send_sem=send, recv_sem=recv, device_id=where, device_id_type=MESH
+    )
+
+
+def greet(peers):
+    barrier = pltpu.get_barrier_semaphore()
+    for peer in peers:
+        pl.semaphore_signal(barrier, inc=1, device_id=peer, device_id_type=MESH)
+    pl.semaphore_wait(barrier, len(peers))
+
+
+def spread_kernel(n, n_fs, n_tp, repeat_dev, x, ssm, query, kv, shift, ows, owa,
+                  xg, w_ssm, w_query, w_kv, shift_g, ows_g, owa_g,
+                  held_x, held_w, held_s, held_o, held_p,
+                  x_send, x_recv, xp_send, xp_recv, w_send, w_recv, f_send, f_recv,
+                  s_send, s_recv, o_send, o_recv, in_sem, out_sem):
+    k = lax.axis_index("sp")
+    f = lax.axis_index("fs")
+    t = lax.axis_index("tp")
+    tokens, half = x.shape
+    rows = ssm.shape[0]
+    part = rows // n_fs
+    cs, cq = w_ssm.shape[1], w_query.shape[1]
+    groups = shift_g.shape[0]
+    other = 1 - t
+    peers = [{"sp": lax.rem(k + s, n)} for s in range(1, n)]
+    peers += [{"fs": lax.rem(f + d, n_fs)} for d in range(1, n_fs)]
+    peers += [{"tp": other}]
+    greet(peers)
+    order = sorted(range(1, n), key=lambda s: -min(s, n - s))
+
+    def piece(which, place, span):
+        if which == 0:
+            return ssm.at[span, pl.ds(pl.multiple_of(place * cs, 128), cs)]
+        if which == 1:
+            return query.at[span, pl.ds(pl.multiple_of(place * cq, 128), cq)]
+        return kv.at[lax.div(place, repeat_dev), span]
+
+    dests = (w_ssm, w_query, w_kv)
+
+    def x_at(j, side):
+        return xg.at[pl.ds(pl.multiple_of(j * tokens, 128), tokens),
+                     pl.ds(pl.multiple_of(side * half, 128), half)]
+
+    copies = []
+    for s in order:
+        peer = lax.rem(k + s, n)
+        for which in range(3):
+            mine = pl.ds(pl.multiple_of(f * part, 16), part)
+            into = pl.ds(pl.multiple_of(k * rows + f * part, 16), part)
+            copies.append(remote(piece(which, peer, mine), dests[which].at[into],
+                                 w_send.at[which, s - 1], w_recv.at[which, s - 1], sp=peer))
+            copies[-1].start()
+    partner = [remote(x, x_at(k, t), xp_send.at[0], xp_recv.at[0], tp=other)]
+    partner[0].start()
+    x_copies = {}
+    for s in order:
+        peer = lax.rem(k + s, n)
+        x_copies[s] = remote(x, x_at(k, t), x_send.at[s - 1], x_recv.at[s - 1], sp=peer)
+        x_copies[s].start()
+        c = remote(shift.at[pl.ds(pl.multiple_of(peer * groups, 8), groups)],
+                   shift_g.at[:, pl.ds(pl.multiple_of(k * tokens, 128), tokens)],
+                   s_send.at[s - 1], s_recv.at[s - 1], sp=peer)
+        c.start()
+        copies.append(c)
+    o_rows = pl.ds(pl.multiple_of(t * ows.shape[0], 16), ows.shape[0])
+    for i, (src, dst) in enumerate(((ows, ows_g), (owa, owa_g))):
+        c = remote(src, dst.at[o_rows], o_send.at[i], o_recv.at[i], tp=other)
+        c.start()
+        copies.append(c)
+    everything = pl.ds(0, rows)
+    here = pl.ds(pl.multiple_of(k * rows, 16), rows)
+    local = [(x, held_x, x_at(k, t))]
+    for which in range(3):
+        local.append((piece(which, k, everything), held_w.at[which], dests[which].at[here]))
+    local.append((shift.at[pl.ds(pl.multiple_of(k * groups, 8), groups)], held_s,
+                  shift_g.at[:, pl.ds(pl.multiple_of(k * tokens, 128), tokens)]))
+    local.append((ows, held_o, ows_g.at[o_rows]))
+    local.append((owa, held_p, owa_g.at[o_rows]))
+    ins = [pltpu.make_async_copy(a, b, in_sem.at[i]) for i, (a, b, _) in enumerate(local)]
+    outs = [pltpu.make_async_copy(b, c, out_sem.at[i]) for i, (_, b, c) in enumerate(local)]
+    for c in ins:
+        c.start()
+    for a, b in zip(ins, outs):
+        a.wait()
+        b.start()
+    forwards = []
+    for i, s in enumerate(sorted(range(1, n), key=lambda s: min(s, n - s))):
+        source = lax.rem(k + n - s, n)
+        into = pl.ds(pl.multiple_of(source * rows + f * part, 16), part)
+        for which in range(3):
+            got = dests[which].at[into]
+            remote(got, got, w_send.at[which, s - 1], w_recv.at[which, s - 1], sp=source).wait_recv()
+            for d in range(1, n_fs):
+                c = remote(got, got, f_send.at[which, s - 1, d - 1], f_recv.at[which, s - 1, d - 1],
+                           fs=lax.rem(f + d, n_fs))
+                c.start()
+                forwards.append(c)
+    for s in sorted(range(1, n), key=lambda s: min(s, n - s)):
+        x_copies[s].wait_recv()
+        block = x_at(lax.rem(k + n - s, n), t)
+        c = remote(block, block, xp_send.at[s], xp_recv.at[s], tp=other)
+        c.start()
+        partner.append(c)
+    for c in copies:
+        c.wait_send()
+    for c in copies[3 * (n - 1):]:
+        c.wait_recv()
+    for c in x_copies.values():
+        c.wait_send()
+    for c in partner + forwards:
+        c.wait()
+    for c in outs:
+        c.wait()
+
+
+def spread(n, n_fs, n_tp, repeat_dev, x, ssm, query, kv, shift, ows, owa):
+    tokens, half = x.shape
+    rows = ssm.shape[0]
+    cs, cq, ck = ssm.shape[1] // n, query.shape[1] // n, kv.shape[2]
+    groups = shift.shape[0] // n
+    bf = jnp.bfloat16
+    dma = pltpu.SemaphoreType.DMA
+    return pl.pallas_call(
+        functools.partial(spread_kernel, n, n_fs, n_tp, repeat_dev),
+        out_shape=[
+            jax.ShapeDtypeStruct((n * tokens, n_tp * half), bf),
+            jax.ShapeDtypeStruct((n * rows, cs), bf),
+            jax.ShapeDtypeStruct((n * rows, cq), bf),
+            jax.ShapeDtypeStruct((n * rows, ck), bf),
+            jax.ShapeDtypeStruct((groups, n * tokens), jnp.float32),
+            jax.ShapeDtypeStruct((n_tp * ows.shape[0], ows.shape[1]), bf),
+            jax.ShapeDtypeStruct((n_tp * owa.shape[0], owa.shape[1]), bf),
+        ],
+        in_specs=[ANY] * 7,
+        out_specs=[ANY] * 7,
+        scratch_shapes=[
+            pltpu.VMEM(x.shape, bf),
+            pltpu.VMEM((3, rows, cs), bf),
+            pltpu.VMEM((groups, tokens), jnp.float32),
+            pltpu.VMEM(ows.shape, bf),
+            pltpu.VMEM(owa.shape, bf),
+            dma((n - 1,)), dma((n - 1,)), dma((n,)), dma((n,)),
+            dma((3, n - 1)), dma((3, n - 1)),
+            dma((3, n - 1, n_fs - 1)), dma((3, n - 1, n_fs - 1)),
+            dma((n - 1,)), dma((n - 1,)), dma((2,)), dma((2,)), dma((7,)), dma((7,)),
+        ],
+        compiler_params=pltpu.CompilerParams(collective_id=0, has_side_effects=True),
+    )(x, ssm, query, kv, shift, ows, owa)
+
+
+def join_kernel(n, hs, ha, gs, ga, held, send, recv, in_sem, out_sem):
+    k = lax.axis_index("sp")
+    t = lax.axis_index("tp")
+    width = hs.shape[2]
+    pairs = [(s, r) for s in range(n) for r in range(2) if (s, r) != (0, 0)]
+    pairs = sorted(pairs, key=lambda p: -min(p[0], n - p[0]))
+    greet([{"sp": lax.rem(k + s, n), "tp": lax.rem(t + r, 2)} for s, r in pairs])
+    columns = pl.ds(pl.multiple_of((t * n + k) * width, 128), width)
+    copies = []
+    for s, r in pairs:
+        for i, (src, dst) in enumerate(((hs, gs), (ha, ga))):
+            side = lax.rem(t + r, 2)
+            c = remote(src.at[side], dst.at[:, columns], send.at[i, s, r], recv.at[i, s, r],
+                       sp=lax.rem(k + s, n), tp=side)
+            c.start()
+            copies.append(c)
+    for i, (src, dst) in enumerate(((hs, gs), (ha, ga))):
+        c = pltpu.make_async_copy(src.at[t], held.at[i], in_sem.at[i])
+        c.start()
+        c.wait()
+        c = pltpu.make_async_copy(held.at[i], dst.at[:, columns], out_sem.at[i])
+        c.start()
+        c.wait()
+    for c in copies:
+        c.wait()
+
+
+def join(n, hs, ha):
+    _, rows, width = hs.shape
+    dma = pltpu.SemaphoreType.DMA
+    return pl.pallas_call(
+        functools.partial(join_kernel, n),
+        out_shape=[jax.ShapeDtypeStruct((rows, 2 * n * width), jnp.bfloat16)] * 2,
+        in_specs=[ANY] * 2,
+        out_specs=[ANY] * 2,
+        scratch_shapes=[pltpu.VMEM((2, rows, width), jnp.bfloat16),
+                        dma((2, n, 2)), dma((2, n, 2)), dma((2,)), dma((2,))],
+        compiler_params=pltpu.CompilerParams(collective_id=1, has_side_effects=True),
+    )(hs, ha)
+
+
+def settle_kernel(n, src, out, held, send, recv, in_sem, out_sem):
+    k = lax.axis_index("sp")
+    rows, width = src.shape[0] // n, src.shape[1]
+    order = sorted(range(1, n), key=lambda s: -min(s, n - s))
+    greet([{"sp": lax.rem(k + s, n)} for s in order])
+    columns = pl.ds(pl.multiple_of(k * width, 128), width)
+    copies = []
+    for s in order:
+        peer = lax.rem(k + s, n)
+        c = remote(src.at[pl.ds(pl.multiple_of(peer * rows, 16), rows)], out.at[:, columns],
+                   send.at[s], recv.at[s], sp=peer)
+        c.start()
+        copies.append(c)
+    c = pltpu.make_async_copy(src.at[pl.ds(pl.multiple_of(k * rows, 16), rows)], held, in_sem.at[0])
+    c.start()
+    c.wait()
+    c = pltpu.make_async_copy(held, out.at[:, columns], out_sem.at[0])
+    c.start()
+    c.wait()
+    for c in copies:
+        c.wait()
+
+
+def settle(n, mixed):
+    rows, width = mixed.shape[0] // n, mixed.shape[1]
+    dma = pltpu.SemaphoreType.DMA
+    return pl.pallas_call(
+        functools.partial(settle_kernel, n),
+        out_shape=jax.ShapeDtypeStruct((rows, n * width), jnp.bfloat16),
+        in_specs=[ANY],
+        out_specs=ANY,
+        scratch_shapes=[pltpu.VMEM((rows, width), jnp.bfloat16), dma((n,)), dma((n,)), dma((1,)), dma((1,))],
+        compiler_params=pltpu.CompilerParams(collective_id=2, has_side_effects=True),
+    )(mixed)
+
+
+def recurrence(drive_in, shift_cols, decay_rate, rotation, input_parts, output_parts, skip_scale):
+    length = drive_in.shape[0]
+    groups, state_dim = decay_rate.shape
+    highest = lax.Precision.HIGHEST
+    drive_cols = jnp.transpose(drive_in).reshape(groups, GROUP_CH, length)
+    in_matrix = input_matrix(decay_rate, rotation, input_parts)
+    drive = jnp.einsum("gqh,ght->gqt", in_matrix, drive_cols, preferred_element_type=jnp.float32)
+    blocks = length // BLOCK
+    triangle = (
+        jnp.arange(BLOCK, dtype=jnp.int32)[:, None] <= jnp.arange(BLOCK, dtype=jnp.int32)[None, :]
+    ).astype(jnp.float32)
+    offsets = jnp.arange(BLOCK, dtype=jnp.float32)
+    centre = BLOCK // 2
+    read_re = output_parts[0].astype(jnp.float32)
+    read_im = output_parts[1].astype(jnp.float32)
+    angle = rotation[:, :, None] * (offsets - centre)[None, None, :]
+    cos_angle = jnp.cos(angle)
+    sin_angle = jnp.sin(angle)
+    phase = rotation[:, :, None] * (offsets + 1.0)[None, None, :]
+    cos_phase = jnp.cos(phase)
+    sin_phase = jnp.sin(phase)
+    carry_re = jnp.zeros((groups, state_dim), jnp.float32)
+    carry_im = carry_re
+    results = []
+    for block in range(blocks):
+        span = slice(block * BLOCK, (block + 1) * BLOCK)
+        part_re = drive[:, :state_dim, span]
+        part_im = drive[:, state_dim:, span]
+        level = jnp.dot(shift_cols[:, span], triangle, precision=highest)
+        log_from = level[:, None, :] - decay_rate[:, :, None] * (offsets + 1.0)[None, None, :]
+        relative = log_from - log_from[:, :, centre : centre + 1]
+        shrink = jnp.exp(-relative)
+        lift_re = shrink * (part_re * cos_angle + part_im * sin_angle)
+        lift_im = shrink * (part_im * cos_angle - part_re * sin_angle)
+        prefix_re = jnp.dot(lift_re.reshape(groups * state_dim, BLOCK), triangle, precision=highest)
+        prefix_im = jnp.dot(lift_im.reshape(groups * state_dim, BLOCK), triangle, precision=highest)
+        prefix_re = prefix_re.reshape(groups, state_dim, BLOCK)
+        prefix_im = prefix_im.reshape(groups, state_dim, BLOCK)
+        grow = jnp.exp(relative)
+        from_start = jnp.exp(log_from)
+        keep_re = from_start * cos_phase
+        keep_im = from_start * sin_phase
+        state_re = grow * (prefix_re * cos_angle - prefix_im * sin_angle)
+        state_im = grow * (prefix_im * cos_angle + prefix_re * sin_angle)
+        state_re = state_re + keep_re * carry_re[:, :, None] - keep_im * carry_im[:, :, None]
+        state_im = state_im + keep_re * carry_im[:, :, None] + keep_im * carry_re[:, :, None]
+        result = jnp.einsum("ghp,gpt->ght", read_re, state_re, precision=highest)
+        result = result - jnp.einsum("ghp,gpt->ght", read_im, state_im, precision=highest)
+        result = result + skip_scale[:, :, None] * drive_cols[:, :, span].astype(jnp.float32)
+        carry_re, carry_im = state_re[:, :, -1], state_im[:, :, -1]
+        results.append(jax.nn.gelu(result).astype(jnp.bfloat16))
+    return jnp.transpose(jnp.concatenate(results, axis=2).reshape(groups * GROUP_CH, length))
+
+
+def fast_body(
+    inputs, norm_gain, in_ssm, in_query, in_key, in_value, decay_rate, rotation, input_parts,
+    output_parts, skip_scale, decay_shift, sink_logit, out_state, out_attend,
+):
+    n, n_fs, n_tp = lax.axis_size("sp"), lax.axis_size("fs"), lax.axis_size("tp")
+    k = lax.axis_index("sp")
+    key_heads = in_key.shape[1] // HEAD_DIM
+    query_heads = in_query.shape[1] // HEAD_DIM
+    heads = query_heads // n
+    rows = in_key.shape[0]
+    kv = jnp.concatenate(
+        [in_key.reshape(rows, key_heads, HEAD_DIM), in_value.reshape(rows, key_heads, HEAD_DIM)], axis=2
+    ).transpose(1, 0, 2)
+    gathered, w_ssm, w_query, w_kv, shift_cols, ows, owa = spread(
+        n, n_fs, n_tp, n // key_heads, inputs, in_ssm, in_query, kv,
+        jnp.transpose(decay_shift), out_state, out_attend,
+    )
+    length = gathered.shape[0]
+    widened = gathered.astype(jnp.float32)
+    scale = lax.rsqrt(jnp.mean(widened * widened, axis=1, keepdims=True) + epsilon)
+    normed = (widened * scale * norm_gain).astype(jnp.bfloat16)
+    drive_in, queries, kv_cols = [
+        jnp.dot(normed, w, preferred_element_type=jnp.float32).astype(jnp.bfloat16)
+        for w in (w_ssm, w_query, w_kv)
+    ]
+
+    def own(array, axis):
+        size = array.shape[axis] // n
+        return lax.dynamic_slice_in_dim(array, k * size, size, axis)
+
+    state_out = recurrence(
+        drive_in, shift_cols, own(decay_rate, 0), own(rotation, 0), own(input_parts, 1),
+        own(output_parts, 1), own(skip_scale, 0),
+    )
+    count = length // WINDOW
+
+    def windows(flat):
+        split = jnp.concatenate([jnp.zeros((WINDOW, HEAD_DIM), flat.dtype), flat], axis=0)
+        split = split.reshape(count + 1, WINDOW, 1, HEAD_DIM)
+        return jnp.concatenate([split[:-1], split[1:]], axis=1)
+
+    attended = window_attention(
+        queries.reshape(count, WINDOW, 1, heads, HEAD_DIM),
+        windows(kv_cols[:, :HEAD_DIM]),
+        windows(kv_cols[:, HEAD_DIM:]),
+        jnp.arange(count, dtype=jnp.int32) * WINDOW,
+        own(sink_logit, 0),
+    )
+    attend_out = attended.reshape(length, heads * HEAD_DIM)
+    tokens = length // n
+
+    def by_side(flat):
+        split = flat.reshape(n, n_tp, tokens // n_tp, flat.shape[1])
+        return split.transpose(1, 0, 2, 3).reshape(n_tp, length // n_tp, flat.shape[1])
+
+    all_state, all_attend = join(n, by_side(state_out), by_side(attend_out))
+    result = jnp.dot(all_state, ows, preferred_element_type=jnp.float32)
+    result = result + jnp.dot(all_attend, owa, preferred_element_type=jnp.float32)
+    return settle(n, result.astype(jnp.bfloat16))
+
+
+def body(*args):
+    n, n_fs, n_tp = lax.axis_size("sp"), lax.axis_size("fs"), lax.axis_size("tp")
+    inputs, in_ssm, in_query, in_key, decay_rate = args[0], args[2], args[3], args[4], args[6]
+    key_heads = in_key.shape[1] // HEAD_DIM
+    query_heads = in_query.shape[1] // HEAD_DIM
+    fits = (
+        n_tp == 2
+        and 1 < n <= 8
+        and n_fs > 1
+        and n % key_heads == 0
+        and query_heads % n == 0
+        and in_ssm.shape[1] == in_query.shape[1]
+        and in_ssm.shape[1] % (128 * n) == 0
+        and 2 * HEAD_DIM == in_ssm.shape[1] // n
+        and decay_rate.shape[0] % (8 * n) == 0
+        and decay_rate.shape[0] * GROUP_CH == in_ssm.shape[1]
+        and inputs.shape[0] % 128 == 0
+        and inputs.shape[1] % 128 == 0
+        and in_ssm.shape[0] % (16 * n_fs) == 0
+        and args[13].shape[1] % 128 == 0
+    )
+    return (fast_body if fits else general_body)(*args)
+
+
 def solution(mesh):
     return jax.shard_map(
         body,

time: 229 us -> 132 us (0.58)
  blocking collectives: 103 us -> 0 us
  Pallas kernels: 0 us -> 75.1 us
  waiting for transfers between devices: 60.3 us -> 0 us
  local copies, waits for them, and re-layouts: 1.27 us -> 14.4 us
  between operations: 13.4 us -> 0.52 us
  matrix products: 40 us -> 34.3 us
  starting transfers between devices: 4.06 us -> 0 us
    all_gather x7 -> x0, blocking collectives: 103 us -> none  [the longest x4 54.7 us: prefix(): lax.all_gather(a.astype(kind), axis)]
    pallas_call x0 -> x3, Pallas kernels: none -> 75.1 us  [the longest x1 36.4 us: spread(): pl.pallas_call(functools.partial(spread_kernel, n, n_fs, n_tp, repeat_dev...]
    all_gather x4 -> x0, waiting for transfers between devices: 51.3 us -> none  [the longest x1 26 us: body(): lax.all_gather(in_ssm, 'sp', axis=0, tiled=True)]
    dot_general x12 -> x26, matrix products: 39.3 us -> 30.9 us  [the longest x4 11.3 us: recurrence(): jnp.dot(lift_im.reshape(groups * state_dim, BLOCK), triangle, precision=h...]
    reduce_scatter x1 -> x0, waiting for transfers between devices: 6.88 us -> none  [body(): lax.psum_scatter((result + jnp.dot(attend_out, column_attend, preferred_e...]
    unnamed x21 -> x27, local copies, waits for them, and re-layouts: 0.12 us -> 4.88 us
    slice x2 -> x20, local copies, waits for them, and re-layouts: 0.82 us -> 5.46 us  [the longest x9 2.84 us: windows(): return jnp.concatenate([split[:-1], split[1:]], axis=1)]
    ppermute x2 -> x0, starting transfers between devices: 3.91 us -> none  [from_behind(): lax.ppermute(value, axis, [(source, source + steps) for source in range(i...]
  transfers between devices with their start and end apart: 7 -> 0, of which waited for: 3 -> 0; matrix products, arithmetic and copies ran while one was open for 20% -> 0% of each run, Pallas kernels for 0% -> 0%
where the time goes in v1:
time: 132 us; the launch traced here: 131 us
  Pallas kernels  75.1 us (57%)
  matrix products  34.3 us (26%)
  local copies, waits for them, and re-layouts  14.4 us (11%)
  other arithmetic  7.03 us (5%)
    pallas_call x1, Pallas kernels, spread(): pl.pallas_call(functools.partial(spread_kernel, n, n_fs, n_tp, repeat_dev...  36.4 us
    pallas_call x1, Pallas kernels, join(): pl.pallas_call(functools.partial(join_kernel, n), out_shape=[jax.ShapeDty...  25 us
    pallas_call x1, Pallas kernels, settle(): pl.pallas_call(functools.partial(settle_kernel, n), out_shape=jax.ShapeDt...  13.8 us
    dot_general x4, matrix products, recurrence(): jnp.dot(lift_im.reshape(groups * state_dim, BLOCK), triangle, precision=h...  11.3 us
    dot_general x4, matrix products, recurrence(): jnp.dot(lift_re.reshape(groups * state_dim, BLOCK), triangle, precision=h...  5.39 us
    unnamed x27, local copies, waits for them, and re-layouts  4.88 us
    dot_general x4, matrix products, recurrence(): jnp.einsum('ghp,gpt->ght', read_im, state_im, precision=highest)  3.82 us
    dot_general x3, matrix products, fast_body(): jnp.dot(normed, w, preferred_element_type=jnp.float32).astype(jnp.bfloat16)  3.41 us

profile of v1, /device:TPU:0, one launch (start us, length us, event | category | flops | bytes accessed | tf_op | source)
XLA Modules:
  0.0 131.3 jit_solution(14337565267041742647)
XLA Ops:
  0.0 1.0 copy.24
  1.2 1.0 copy.25
  2.4 0.9 maximum_bitcast_fusion.kv
  3.3 36.4 %shard_map.145 = (bf16[512,2048]{1,0:T(8,128)(2,1)}, bf16[2048,128]{1,0:T(8,128)(2,1)}, bf16[2048,128]{1,0:T(8,128)(2,1)}, bf16[2048,128]{1,0:T(8,128)(2,1)}, f3...) custom-call(bf16[128,1024]{1,0:T(8,128)(2,1)} %x.5, bf16[512,512]{1,0:T(8,128)(2,1)} %ssm.1, ...), custom_call_target="tpu_custom_call" | custom-call | tf_op jit(solution)/shard_map/pallas_call | solution.py:393
  39.7 2.2 %fusion = f32[512]{0:T(512)S(1)} fusion(bf16[512,2048]{1,0:T(8,128)(2,1)} %get-tuple-element.16), kind=kLoop, calls=%fused_computation.2 | loop fusion | flops 3145216 | bytes 2099200 | tf_op jit(solution)/shard_map/reduce_sum | solution.py:571
  41.9 0.5 fusion.2
  42.5 0.5 copy-done.6
  43.0 0.8 convolution_convert_fusion.2
  43.8 0.6 pad_slice_fusion
  44.5 0.6 copy.34
  45.2 0.7 convolution_convert_fusion.1
  45.9 0.8 reshape.206
  47.1 0.6 copy-done.4
  47.7 1.4 %fusion.316 = (f32[4,2,128]{2,1,0:T(2,128)S(1)}, f32[4,1,2,128,256]{3,4,2,0,1:T(8,128)S(1)}) fusion(bf16[4,128,2,64]{3,2,1,0:T(2,128)(2,1)} %reshape.206, bf16[4,128,1,64]{1,3,0,2:T(8,128)(2,1)} %copy.34, bf16[4,128,1,64]{1,3,0,2:T(8,128)(2,1)S(1)} %copy.33, pred[4,128,256]{1,2,0:T(8,128)(4,1)S(1)} %broadcast_and_fusion), kind=kOutput, calls=%fused_computation.351 | convolution fusion | flops 34601984 | bytes 1445888 | tf_op jit(solution)/shard_map/nqgrd,nkgd->ngrqk/dot_general | solution.py:74
  49.2 1.1 fusion.11
  50.4 0.9 slice.148
  51.3 0.6 copy.31
  52.0 2.0 %fusion.6 = bf16[4,128,1,2,64]{1,4,3,0,2:T(8,128)(2,1)} fusion(f32[4,1,2,128,256]{3,4,2,0,1:T(8,128)S(1)} %get-tuple-element.40, f32[4,2,128]{2,1,0:T(2,128)S(1)} %exponential_add_fusion, f32[4,2,128]{2,1,0:T(2,128)S(1)} %broadcast_maximum_fusion, pred[4,128,256]{1,2,0:T(8,128)(4,1)} %copy-done.4, bf16[4,128,1,64]{1,3,0,2:T(8,128)(2,1)S(1)} %copy.32, ...), kind=kOutput, calls=%fused_computation.14 | convolution fusion | flops 34930688 | bytes 1449984 | tf_op jit(solution)/shard_map/ngrqk,nkgd->nqgrd/dot_general | solution.py:90
  54.0 1.0 reshape.207
  55.0 0.8 copy.46
  55.8 0.7 fusion.301
  56.6 0.8 fusion.239
  57.4 1.9 %convolution_convert_fusion.3 = bf16[128,512]{1,0:T(8,128)(2,1)S(1)} fusion(bf16[2048,128]{1,0:T(8,128)(2,1)} %get-tuple-element.15, bf16[512,2048]{1,0:T(8,128)(2,1)S(1)} %fusion.2), kind=kOutput, calls=%fused_computation.13 | convolution fusion | flops 268500992 | bytes 2752512 | tf_op jit(solution)/shard_map/dot_general | solution.py:574
  59.3 0.7 fusion.291
  60.4 0.3 slice_reduce_fusion.9
  60.6 1.3 fusion.55
  62.1 3.3 %fusion.64 = (f32[8,64,128]{2,1,0:T(8,128)S(1)}, f32[8,64,128]{2,1,0:T(8,128)S(1)}, f32[8,64,128]{2,1,0:T(8,128)S(1)}) fusion(f32[8,64,128]{2,1,0:T(8,128)S(1)} %fusion.55, f32[128]{0:T(128)S(1)} %get-tuple-element.41, f32[8,64]{1,0:T(8,128)S(1)} %get-tuple-element.24, f32[8,64]{1,0:T(8,128)S(1)} %slice_reduce_fusion.9, f32[128]{0:T(128)S(1)} %get-tuple-element.42, ...), kind=kOutput, calls=%fused_computation.84 | convolution fusion | flops 102711296 | bytes 1611776 | tf_op jit(solution)/shard_map/dot_general | solution.py:533
  66.0 0.3 slice_reduce_fusion.8
  66.3 1.5 %fusion.71 = f32[8,64,128]{2,1,0:T(8,128)S(1)} fusion(f32[8,128,512]{2,1,0:T(8,128)S(1)} %fusion.291, f32[8,64]{1,0:T(8,128)S(1)} %slice_reduce_fusion.8, f32[8,128]{1,0:T(8,128)S(1)} %fusion.279, f32[128]{0:T(128)S(1)} %get-tuple-element.41, f32[8,64]{1,0:T(8,128)S(1)} %get-tuple-element.24, f32[128]{0:T(128)S(1)} %get-tuple-element.42, ...), kind=kOutput, calls=%fused_computation.91 | convolution fusion | flops 101269504 | bytes 803840 | tf_op jit(solution)/shard_map/dot_general | solution.py:532
  67.8 0.3 slice_reduce_fusion.6
  68.4 3.3 %fusion.80 = (f32[8,64,128]{2,1,0:T(8,128)S(1)}, f32[8,64,128]{2,1,0:T(8,128)S(1)}, f32[8,64,128]{2,1,0:T(8,128)S(1)}) fusion(f32[8,64,128]{2,1,0:T(8,128)S(1)} %fusion.71, f32[8,64]{1,0:T(8,128)S(1)} %slice_reduce_fusion.6, f32[8,64]{1,0:T(8,128)S(1)} %slice_reduce_fusion.7, f32[8,64]{1,0:T(8,128)S(1)} %slice_reduce_fusion.8, f32[8,128]{1,0:T(8,128)S(1)} %fusion.279, ...), kind=kOutput, calls=%fused_computation.98 | convolution fusion | flops 102842368 | bytes 1619968 | tf_op jit(solution)/shard_map/dot_general | solution.py:533
  72.0 0.3 fusion.257
  72.5 1.3 fusion.87
  73.8 0.3 slice_reduce_fusion.3
  74.5 3.3 %fusion.96 = (f32[8,64,128]{2,1,0:T(8,128)S(1)}, f32[8,64,128]{2,1,0:T(8,128)S(1)}, f32[8,64,128]{2,1,0:T(8,128)S(1)}) fusion(f32[8,64,128]{2,1,0:T(8,128)S(1)} %fusion.87, f32[8,64]{1,0:T(8,128)S(1)} %slice_reduce_fusion.3, f32[8,64]{1,0:T(8,128)S(1)} %slice_reduce_fusion.4, f32[8,64]{1,0:T(8,128)S(1)} %slice_reduce_fusion.5, f32[8,128]{1,0:T(8,128)S(1)} %fusion.278, ...), kind=kOutput, calls=%fused_computation.112 | convolution fusion | flops 102842368 | bytes 1619968 | tf_op jit(solution)/shard_map/dot_general | solution.py:533
  78.0 0.3 fusion.265
  78.6 1.3 fusion.103
  79.9 1.5 %fusion.107 = f32[8,64,128]{2,1,0:T(8,128)S(1)} fusion(f32[8,128,512]{2,1,0:T(8,128)S(1)} %fusion.291, f32[8,64]{1,0:T(8,128)S(1)} %slice_reduce_fusion.2, f32[8,128]{1,0:T(8,128)S(1)} %fusion.280, f32[128]{0:T(128)S(1)} %get-tuple-element.41, f32[8,64]{1,0:T(8,128)S(1)} %get-tuple-element.24, f32[128]{0:T(128)S(1)} %get-tuple-element.42, ...), kind=kOutput, calls=%fused_computation.122 | convolution fusion | flops 101269504 | bytes 803840 | tf_op jit(solution)/shard_map/dot_general | solution.py:533
  81.4 0.3 slice_reduce_fusion
  81.7 0.3 slice_reduce_fusion.1
  82.0 2.3 %fusion.113 = f32[8,16,128]{2,1,0:T(8,128)S(1)} fusion(f32[8,64,128]{2,1,0:T(8,128)S(1)} %fusion.107, f32[8,64,128]{2,1,0:T(8,128)S(1)} %fusion.103, f32[8,64]{1,0:T(8,128)S(1)} %slice_reduce_fusion, f32[8,64]{1,0:T(8,128)S(1)} %slice_reduce_fusion.1, f32[8,64]{1,0:T(8,128)S(1)} %slice_reduce_fusion.2, f32[8,128]{1,0:T(8,128)S(1)} %fusion.280, ...), kind=kOutput, calls=%fused_computation.127 | convolution fusion | flops 13565952 | bytes 648196 | tf_op jit(solution)/shard_map/ghp,gpt->ght/dot_general | solution.py:544
  84.3 3.0 %fusion.275 = bf16[8,16,128]{2,1,0:T(8,128)(2,1)S(1)} fusion(f32[8,16,128]{2,1,0:T(8,128)S(1)} %fusion.113, f32[8,64,128]{2,1,0:T(8,128)S(1)} %fusion.103, f32[8,64,128]{2,1,0:T(8,128)S(1)} %fusion.107, f32[8,64]{1,0:T(8,128)S(1)} %slice_reduce_fusion, f32[8,64]{1,0:T(8,128)S(1)} %slice_reduce_fusion.1, f32[8,64]{1,0:T(8,128)S(1)} %slice_reduce_fusion.2, ...), kind=kOutput, calls=%fused_computation.299 | convolution fusion | flops 13778944 | bytes 717832 | tf_op jit(solution)/shard_map/ghp,gpt->ght/dot_general | solution.py:545
  87.5 0.7 copy.30
  88.1 25.0 %shard_map.146 = (bf16[256,1024]{1,0:T(8,128)(2,1)}, bf16[256,1024]{1,0:T(8,128)(2,1)}) custom-call(bf16[2,256,128]{2,1,0:T(8,128)(2,1)} %bitcast.124, bf16[2,256,128]{2,1,0:T(8,128)(2,1)} %bitcast.120), custom_call_target="tpu_custom_call" | custom-call | tf_op jit(solution)/shard_map/pallas_call | solution.py:451
  113.2 1.5 %fusion.317 = f32[256,512]{1,0:T(8,128)S(1)} fusion(bf16[256,1024]{1,0:T(8,128)(2,1)} %get-tuple-element.19, bf16[1024,512]{1,0:T(8,128)(2,1)S(1)} %copy-done.3), kind=kOutput, calls=%fused_computation.352 | convolution fusion | flops 268435456 | bytes 2097152 | tf_op jit(solution)/shard_map/dot_general | solution.py:608
  114.7 1.1 fusion.5.src
  115.9 13.8 %shard_map.147 = bf16[64,2048]{1,0:T(8,128)(2,1)} custom-call(bf16[256,512]{1,0:T(8,128)(2,1)} %fusion.5.src), custom_call_target="tpu_custom_call" | custom-call | tf_op jit(solution)/shard_map/pallas_call | solution.py:488
  129.6 1.7 %copy.52 = bf16[64,2048]{1,0:T(8,128)(2,1)} copy(bf16[64,2048]{1,0:T(8,128)(2,1)} %shard_map.147) | data formatting | bytes 524288
  (58 shorter events, 4.1 us)
Async XLA Ops:
  0.0 65.3 %copy-start = (bf16[2,32,16,64]{3,2,1,0:T(8,128)(2,1)S(1)}, bf16[2,32,16,64]{3,2,1,0:T(8,128)(2,1)}, u32[]{:S(2)}) copy-start(bf16[2,32,16,64]{3,2,1,0:T(8,128)(2,1)} %param.24) | copy-start | bytes 393220
  3.3 38.6 %copy-start.8 = (f32[2048]{0:T(1024)S(1)}, f32[2048]{0:T(1024)}, u32[]{:S(2)}) copy-start(f32[2048]{0:T(1024)} %param.16) | copy-start | bytes 24580
  39.7 2.3 %copy-start.1 = (bf16[512,2048]{1,0:T(8,128)(2,1)S(1)}, bf16[512,2048]{1,0:T(8,128)(2,1)}, u32[]{:S(2)}) copy-start(bf16[512,2048]{1,0:T(8,128)(2,1)} %get-tuple-element.16) | copy-start | bytes 6291460
  41.9 1.0 copy-start.6
  42.5 2.7 %copy-start.5 = (bf16[2048,128]{1,0:T(8,128)(2,1)S(1)}, bf16[2048,128]{1,0:T(8,128)(2,1)}, u32[]{:S(2)}) copy-start(bf16[2048,128]{1,0:T(8,128)(2,1)} %get-tuple-element.18) | copy-start | bytes 1572868
  45.2 3.9 %copy-start.11 = (f32[8]{0:T(128)S(1)}, f32[8]{0:T(128)}, u32[]{:S(2)}) copy-start(f32[8]{0:T(128)} %param.27) | copy-start | bytes 100
  47.1 0.6 copy-start.4
  57.4 2.6 %copy-start.10 = (f32[8,512]{1,0:T(8,128)S(1)}, f32[8,512]{1,0:T(8,128)}, u32[]{:S(2)}) copy-start(f32[8,512]{1,0:T(8,128)} %get-tuple-element.14) | copy-start | bytes 49156
  60.4 5.2 %copy-start.9 = (f32[32,16]{0,1:T(8,128)S(1)}, f32[32,16]{0,1:T(8,128)}, u32[]{:S(2)}) copy-start(f32[32,16]{0,1:T(8,128)} %param.25) | copy-start | bytes 6148
  81.9 31.2 %copy-start.3 = (bf16[1024,512]{1,0:T(8,128)(2,1)S(1)}, bf16[1024,512]{1,0:T(8,128)(2,1)}, u32[]{:S(2)}) copy-start(bf16[1024,512]{1,0:T(8,128)(2,1)} %get-tuple-element.20) | copy-start | bytes 3145732
  84.3 30.4 %copy-start.2 = (bf16[1024,512]{1,0:T(8,128)(2,1)S(1)}, bf16[1024,512]{1,0:T(8,128)(2,1)}, u32[]{:S(2)}) copy-start(bf16[1024,512]{1,0:T(8,128)(2,1)} %get-tuple-element.22) | copy-start | bytes 3145732
  113.1 1.6 %copy-start.7 = (bf16[256,1024]{1,0:T(8,128)(2,1)S(1)}, bf16[256,1024]{1,0:T(8,128)(2,1)}, u32[]{:S(2)}) copy-start(bf16[256,1024]{1,0:T(8,128)(2,1)} %get-tuple-element.21) | copy-start | bytes 1572868

commit v2 on v1

--- a/solution.py
+++ b/solution.py
@@ -281,7 +281,7 @@
 def spread_kernel(n, n_fs, n_tp, repeat_dev, x, ssm, query, kv, shift, ows, owa,
                   xg, w_ssm, w_query, w_kv, shift_g, ows_g, owa_g,
                   held_x, held_w, held_s, held_o, held_p,
-                  x_send, x_recv, xp_send, xp_recv, w_send, w_recv, f_send, f_recv,
+                  x_send, x_recv, q_send, q_recv, xp_send, xp_recv, w_send, w_recv, f_send, f_recv,
                   s_send, s_recv, o_send, o_recv, in_sem, out_sem):
     k = lax.axis_index("sp")
     f = lax.axis_index("fs")
@@ -322,16 +322,42 @@
             copies[-1].start()
     partner = [remote(x, x_at(k, t), xp_send.at[0], xp_recv.at[0], tp=other)]
     partner[0].start()
-    x_copies = {}
     for s in order:
         peer = lax.rem(k + s, n)
-        x_copies[s] = remote(x, x_at(k, t), x_send.at[s - 1], x_recv.at[s - 1], sp=peer)
-        x_copies[s].start()
         c = remote(shift.at[pl.ds(pl.multiple_of(peer * groups, 8), groups)],
                    shift_g.at[:, pl.ds(pl.multiple_of(k * tokens, 128), tokens)],
                    s_send.at[s - 1], s_recv.at[s - 1], sp=peer)
         c.start()
         copies.append(c)
+
+    def hop(step, way):
+        block = lax.rem(k - way * step + n, n)
+        dst = x_at(block, t)
+        src = x if step == 0 else dst
+        to = lax.rem(k + way + n, n)
+        i = 0 if way > 0 else 1
+        active = jnp.logical_and(k + way >= 0, k + way < n)
+        active = jnp.logical_and(active, jnp.logical_and(k - way * step >= 0, k - way * step < n))
+        return active, remote(src, dst, x_send.at[i, step], x_recv.at[i, step], sp=to)
+
+    def arrival(step, way):
+        origin = k - way * (step + 1)
+        block = x_at(lax.rem(origin + n, n), t)
+        i = 0 if way > 0 else 1
+        active = jnp.logical_and(origin >= 0, origin < n)
+        c = remote(block, block, x_send.at[i, step], x_recv.at[i, step], sp=lax.rem(k - way + n, n))
+        p = remote(block, block, q_send.at[i, step], q_recv.at[i, step], tp=other)
+        return active, c, p
+
+    def start_hops(step):
+        for way in (1, -1):
+            active, c = hop(step, way)
+
+            @pl.when(active)
+            def _():
+                c.start()
+
+    start_hops(0)
     o_rows = pl.ds(pl.multiple_of(t * ows.shape[0], 16), ows.shape[0])
     for i, (src, dst) in enumerate(((ows, ows_g), (owa, owa_g))):
         c = remote(src, dst.at[o_rows], o_send.at[i], o_recv.at[i], tp=other)
@@ -365,18 +391,35 @@
                            fs=lax.rem(f + d, n_fs))
                 c.start()
                 forwards.append(c)
-    for s in sorted(range(1, n), key=lambda s: min(s, n - s)):
-        x_copies[s].wait_recv()
-        block = x_at(lax.rem(k + n - s, n), t)
-        c = remote(block, block, xp_send.at[s], xp_recv.at[s], tp=other)
-        c.start()
-        partner.append(c)
+    for step in range(n - 1):
+        for way in (1, -1):
+            active, c, p = arrival(step, way)
+
+            @pl.when(active)
+            def _():
+                c.wait_recv()
+                p.start()
+
+        if step + 1 < n - 1:
+            start_hops(step + 1)
+    for step in range(n - 1):
+        for way in (1, -1):
+            active, c = hop(step, way)
+
+            @pl.when(active)
+            def _():
+                c.wait_send()
+
+            active, _c, p = arrival(step, way)
+
+            @pl.when(active)
+            def _():
+                p.wait()
+
     for c in copies:
         c.wait_send()
     for c in copies[3 * (n - 1):]:
         c.wait_recv()
-    for c in x_copies.values():
-        c.wait_send()
     for c in partner + forwards:
         c.wait()
     for c in outs:
@@ -409,7 +452,7 @@
             pltpu.VMEM((groups, tokens), jnp.float32),
             pltpu.VMEM(ows.shape, bf),
             pltpu.VMEM(owa.shape, bf),
-            dma((n - 1,)), dma((n - 1,)), dma((n,)), dma((n,)),
+            dma((2, n - 1)), dma((2, n - 1)), dma((2, n - 1)), dma((2, n - 1)), dma((1,)), dma((1,)),
             dma((3, n - 1)), dma((3, n - 1)),
             dma((3, n - 1, n_fs - 1)), dma((3, n - 1, n_fs - 1)),
             dma((n - 1,)), dma((n - 1,)), dma((2,)), dma((2,)), dma((7,)), dma((7,)),
@@ -495,58 +538,179 @@
     )(mixed)
 
 
-def recurrence(drive_in, shift_cols, decay_rate, rotation, input_parts, output_parts, skip_scale):
-    length = drive_in.shape[0]
-    groups, state_dim = decay_rate.shape
-    highest = lax.Precision.HIGHEST
-    drive_cols = jnp.transpose(drive_in).reshape(groups, GROUP_CH, length)
-    in_matrix = input_matrix(decay_rate, rotation, input_parts)
-    drive = jnp.einsum("gqh,ght->gqt", in_matrix, drive_cols, preferred_element_type=jnp.float32)
+def halves(x):
+    high = x.astype(jnp.bfloat16)
+    return high, (x - high.astype(jnp.float32)).astype(jnp.bfloat16)
+
+
+def split_dot(x, exact):
+    high, low = halves(x)
+    return jnp.dot(high, exact, preferred_element_type=jnp.float32) + jnp.dot(
+        low, exact, preferred_element_type=jnp.float32
+    )
+
+
+def column(row):
+    size = row.shape[1]
+    same = lax.broadcasted_iota(jnp.int32, (size, size), 0) == lax.broadcasted_iota(
+        jnp.int32, (size, size), 1
+    )
+    return jnp.sum(jnp.where(same, row, 0.0), axis=1, keepdims=True)
+
+
+def mixer_kernel(k, x, gain, w_ssm, w_query, w_kv, shift, rate, rotation, in_parts, out_parts,
+                 skip, sinks, hs, ha, u_scr, q_scr, kv_scr, y_scr):
+    f32, bf = jnp.float32, jnp.bfloat16
+    length = x.shape[0]
     blocks = length // BLOCK
-    triangle = (
-        jnp.arange(BLOCK, dtype=jnp.int32)[:, None] <= jnp.arange(BLOCK, dtype=jnp.int32)[None, :]
-    ).astype(jnp.float32)
-    offsets = jnp.arange(BLOCK, dtype=jnp.float32)
+    groups = shift.shape[0]
+    state = rate.shape[1]
+    heads = w_query.shape[1] // HEAD_DIM
+    side = BLOCK // 2
+    kv_scr[0:WINDOW, :] = jnp.zeros((WINDOW, kv_scr.shape[1]), bf)
+
+    for b in range(blocks):
+        span = slice(b * BLOCK, (b + 1) * BLOCK)
+        wide = x[span, :].astype(f32)
+        scale = lax.rsqrt(jnp.mean(wide * wide, axis=1, keepdims=True) + epsilon)
+        normed = (wide * scale * gain[...]).astype(bf)
+        u = jnp.dot(normed, w_ssm[...], preferred_element_type=f32)
+        u_scr[:, span] = jnp.transpose(u.astype(bf).astype(f32))
+        q_scr[span, :] = jnp.dot(normed, w_query[...], preferred_element_type=f32).astype(bf)
+        kv_scr[(b + 1) * BLOCK : (b + 2) * BLOCK, :] = jnp.dot(
+            normed, w_kv[...], preferred_element_type=f32
+        ).astype(bf)
+
+    shape = (BLOCK, BLOCK)
+    upto = lax.broadcasted_iota(jnp.int32, shape, 0) <= lax.broadcasted_iota(jnp.int32, shape, 1)
+    tri = upto.astype(f32).astype(bf)
     centre = BLOCK // 2
-    read_re = output_parts[0].astype(jnp.float32)
-    read_im = output_parts[1].astype(jnp.float32)
-    angle = rotation[:, :, None] * (offsets - centre)[None, None, :]
-    cos_angle = jnp.cos(angle)
-    sin_angle = jnp.sin(angle)
-    phase = rotation[:, :, None] * (offsets + 1.0)[None, None, :]
-    cos_phase = jnp.cos(phase)
-    sin_phase = jnp.sin(phase)
-    carry_re = jnp.zeros((groups, state_dim), jnp.float32)
-    carry_im = carry_re
-    results = []
-    for block in range(blocks):
-        span = slice(block * BLOCK, (block + 1) * BLOCK)
-        part_re = drive[:, :state_dim, span]
-        part_im = drive[:, state_dim:, span]
-        level = jnp.dot(shift_cols[:, span], triangle, precision=highest)
-        log_from = level[:, None, :] - decay_rate[:, :, None] * (offsets + 1.0)[None, None, :]
-        relative = log_from - log_from[:, :, centre : centre + 1]
-        shrink = jnp.exp(-relative)
-        lift_re = shrink * (part_re * cos_angle + part_im * sin_angle)
-        lift_im = shrink * (part_im * cos_angle - part_re * sin_angle)
-        prefix_re = jnp.dot(lift_re.reshape(groups * state_dim, BLOCK), triangle, precision=highest)
-        prefix_im = jnp.dot(lift_im.reshape(groups * state_dim, BLOCK), triangle, precision=highest)
-        prefix_re = prefix_re.reshape(groups, state_dim, BLOCK)
-        prefix_im = prefix_im.reshape(groups, state_dim, BLOCK)
-        grow = jnp.exp(relative)
-        from_start = jnp.exp(log_from)
-        keep_re = from_start * cos_phase
-        keep_im = from_start * sin_phase
-        state_re = grow * (prefix_re * cos_angle - prefix_im * sin_angle)
-        state_im = grow * (prefix_im * cos_angle + prefix_re * sin_angle)
-        state_re = state_re + keep_re * carry_re[:, :, None] - keep_im * carry_im[:, :, None]
-        state_im = state_im + keep_re * carry_im[:, :, None] + keep_im * carry_re[:, :, None]
-        result = jnp.einsum("ghp,gpt->ght", read_re, state_re, precision=highest)
-        result = result - jnp.einsum("ghp,gpt->ght", read_im, state_im, precision=highest)
-        result = result + skip_scale[:, :, None] * drive_cols[:, :, span].astype(jnp.float32)
-        carry_re, carry_im = state_re[:, :, -1], state_im[:, :, -1]
-        results.append(jax.nn.gelu(result).astype(jnp.bfloat16))
-    return jnp.transpose(jnp.concatenate(results, axis=2).reshape(groups * GROUP_CH, length))
+    levels, lifts, grows, starts = [], [], [], []
+    for b in range(blocks):
+        part = shift[:, b * BLOCK : (b + 1) * BLOCK]
+        high, low = halves(part)
+        low2 = (part - high.astype(f32) - low.astype(f32)).astype(bf)
+        level = (
+            jnp.dot(high, tri, preferred_element_type=f32)
+            + jnp.dot(low, tri, preferred_element_type=f32)
+            + jnp.dot(low2, tri, preferred_element_type=f32)
+        )
+        middle = level[:, centre : centre + 1]
+        lifts.append(jnp.exp(middle - level))
+        grows.append(jnp.exp(level - middle))
+        starts.append(jnp.exp(middle))
+    away = lax.broadcasted_iota(jnp.int32, (state, BLOCK), 1).astype(f32) - float(centre)
+    first = k * groups
+    for g in range(groups):
+        rates = column(rate[pl.ds(first + g, 1), :])
+        turns = column(rotation[pl.ds(first + g, 1), :])
+        angle = turns * away
+        cos, sin = jnp.cos(angle), jnp.sin(angle)
+        fade = jnp.exp(-rates * away)
+        rise = jnp.exp(rates * away)
+        up_re, up_im = rise * cos, -(rise * sin)
+        down_re, down_im = fade * cos, fade * sin
+        damped = jnp.exp(-rates)
+        lift_re = damped * jnp.cos(turns) - 1.0
+        lift_im = damped * jnp.sin(turns)
+        modulus = rates * rates + turns * turns
+        factor_re = (turns * lift_im - rates * lift_re) / modulus
+        factor_im = -(turns * lift_re + rates * lift_im) / modulus
+        part_re = in_parts[0, first + g].astype(f32)
+        part_im = in_parts[1, first + g].astype(f32)
+        in_matrix = jnp.concatenate(
+            [factor_re * part_re - factor_im * part_im, factor_re * part_im + factor_im * part_re],
+            axis=0,
+        ).astype(bf)
+        read = jnp.concatenate(
+            [out_parts[0, first + g].astype(f32), -out_parts[1, first + g].astype(f32)], axis=1
+        ).astype(bf)
+        reach = jnp.exp(-rates * (centre + 1.0))
+        reach_re = reach * jnp.cos(turns * (centre + 1.0))
+        reach_im = reach * jnp.sin(turns * (centre + 1.0))
+        u = u_scr[g * GROUP_CH : (g + 1) * GROUP_CH, :]
+        drive = jnp.dot(in_matrix, u.astype(bf), preferred_element_type=f32)
+        lifted = []
+        for b in range(blocks):
+            span = slice(b * BLOCK, (b + 1) * BLOCK)
+            row = lifts[b][g : g + 1, :]
+            d_re, d_im = drive[:state, span] * row, drive[state:, span] * row
+            lifted += [d_re * up_re - d_im * up_im, d_re * up_im + d_im * up_re]
+        prefix = split_dot(jnp.concatenate(lifted, axis=0), tri)
+        carry_re = jnp.zeros((state, 1), f32)
+        carry_im = carry_re
+        skips = column(skip[pl.ds(first + g, 1), :])
+        for b in range(blocks):
+            span = slice(b * BLOCK, (b + 1) * BLOCK)
+            begin = starts[b][g : g + 1, :]
+            base_re = begin * (carry_re * reach_re - carry_im * reach_im)
+            base_im = begin * (carry_re * reach_im + carry_im * reach_re)
+            p_re = prefix[2 * b * state : (2 * b + 1) * state] + base_re
+            p_im = prefix[(2 * b + 1) * state : (2 * b + 2) * state] + base_im
+            row = grows[b][g : g + 1, :]
+            s_re = row * (down_re * p_re - down_im * p_im)
+            s_im = row * (down_re * p_im + down_im * p_re)
+            carry_re, carry_im = s_re[:, BLOCK - 1 :], s_im[:, BLOCK - 1 :]
+            high, low = halves(jnp.concatenate([s_re, s_im], axis=0))
+            y = jnp.dot(read, high, preferred_element_type=f32) + jnp.dot(
+                read, low, preferred_element_type=f32
+            )
+            y_scr[g * GROUP_CH : (g + 1) * GROUP_CH, span] = y + skips * u[:, span]
+
+    for b in range(blocks):
+        y = y_scr[:, b * BLOCK : (b + 1) * BLOCK]
+        y = jnp.transpose(jax.nn.gelu(y)).astype(bf)
+        hs[0, b * side : (b + 1) * side, :] = y[:side]
+        hs[1, b * side : (b + 1) * side, :] = y[side:]
+
+    wide = (WINDOW, 2 * WINDOW)
+    gap = lax.broadcasted_iota(jnp.int32, wide, 0) + WINDOW - lax.broadcasted_iota(jnp.int32, wide, 1)
+    inside = (gap >= 0) & (gap < WINDOW)
+    inside_first = inside & (lax.broadcasted_iota(jnp.int32, wide, 1) >= WINDOW)
+    for b in range(blocks):
+        keys = kv_scr[b * WINDOW : (b + 2) * WINDOW, :HEAD_DIM]
+        values = kv_scr[b * WINDOW : (b + 2) * WINDOW, HEAD_DIM:]
+        valid = inside if b else inside_first
+        outs = []
+        for h in range(heads):
+            query = q_scr[b * WINDOW : (b + 1) * WINDOW, h * HEAD_DIM : (h + 1) * HEAD_DIM]
+            scores = lax.dot_general(query, keys, (((1,), (1,)), ((), ())), preferred_element_type=f32)
+            scores = jnp.where(valid, scores * HEAD_DIM ** (-0.5), floor_score)
+            sink = sinks[k * heads + h]
+            peak = jnp.maximum(jnp.max(scores, axis=1, keepdims=True), sink)
+            raised = jnp.where(valid, jnp.exp(scores - peak), 0.0)
+            total = jnp.sum(raised, axis=1, keepdims=True) + jnp.exp(sink - peak)
+            weights = (raised / total).astype(bf)
+            outs.append(jnp.dot(weights, values, preferred_element_type=f32))
+        out = jnp.concatenate(outs, axis=1).astype(bf)
+        ha[0, b * side : (b + 1) * side, :] = out[:side]
+        ha[1, b * side : (b + 1) * side, :] = out[side:]
+
+
+def mixer_entry(*refs):
+    mixer_kernel(lax.axis_index("sp"), *refs)
+
+
+def mixer(x, gain, w_ssm, w_query, w_kv, shift, rate, rotation, in_parts, out_parts, skip, sinks,
+          entry=mixer_entry, interpret=False):
+    length = x.shape[0]
+    vmem = pl.BlockSpec(memory_space=pltpu.VMEM)
+    return pl.pallas_call(
+        entry,
+        out_shape=[
+            jax.ShapeDtypeStruct((2, length // 2, w_ssm.shape[1]), jnp.bfloat16),
+            jax.ShapeDtypeStruct((2, length // 2, w_query.shape[1]), jnp.bfloat16),
+        ],
+        in_specs=[vmem] * 11 + [pl.BlockSpec(memory_space=pltpu.SMEM)],
+        out_specs=[vmem] * 2,
+        scratch_shapes=[
+            pltpu.VMEM((w_ssm.shape[1], length), jnp.float32),
+            pltpu.VMEM((length, w_query.shape[1]), jnp.bfloat16),
+            pltpu.VMEM((length + WINDOW, w_kv.shape[1]), jnp.bfloat16),
+            pltpu.VMEM((w_ssm.shape[1], length), jnp.float32),
+        ],
+        interpret=interpret,
+    )(x, gain, w_ssm, w_query, w_kv, shift, rate, rotation, in_parts, out_parts, skip, sinks)
 
 
 def fast_body(
@@ -554,10 +718,7 @@
     output_parts, skip_scale, decay_shift, sink_logit, out_state, out_attend,
 ):
     n, n_fs, n_tp = lax.axis_size("sp"), lax.axis_size("fs"), lax.axis_size("tp")
-    k = lax.axis_index("sp")
     key_heads = in_key.shape[1] // HEAD_DIM
-    query_heads = in_query.shape[1] // HEAD_DIM
-    heads = query_heads // n
     rows = in_key.shape[0]
     kv = jnp.concatenate(
         [in_key.reshape(rows, key_heads, HEAD_DIM), in_value.reshape(rows, key_heads, HEAD_DIM)], axis=2
@@ -566,45 +727,11 @@
         n, n_fs, n_tp, n // key_heads, inputs, in_ssm, in_query, kv,
         jnp.transpose(decay_shift), out_state, out_attend,
     )
-    length = gathered.shape[0]
-    widened = gathered.astype(jnp.float32)
-    scale = lax.rsqrt(jnp.mean(widened * widened, axis=1, keepdims=True) + epsilon)
-    normed = (widened * scale * norm_gain).astype(jnp.bfloat16)
-    drive_in, queries, kv_cols = [
-        jnp.dot(normed, w, preferred_element_type=jnp.float32).astype(jnp.bfloat16)
-        for w in (w_ssm, w_query, w_kv)
-    ]
-
-    def own(array, axis):
-        size = array.shape[axis] // n
-        return lax.dynamic_slice_in_dim(array, k * size, size, axis)
-
-    state_out = recurrence(
-        drive_in, shift_cols, own(decay_rate, 0), own(rotation, 0), own(input_parts, 1),
-        own(output_parts, 1), own(skip_scale, 0),
-    )
-    count = length // WINDOW
-
-    def windows(flat):
-        split = jnp.concatenate([jnp.zeros((WINDOW, HEAD_DIM), flat.dtype), flat], axis=0)
-        split = split.reshape(count + 1, WINDOW, 1, HEAD_DIM)
-        return jnp.concatenate([split[:-1], split[1:]], axis=1)
-
-    attended = window_attention(
-        queries.reshape(count, WINDOW, 1, heads, HEAD_DIM),
-        windows(kv_cols[:, :HEAD_DIM]),
-        windows(kv_cols[:, HEAD_DIM:]),
-        jnp.arange(count, dtype=jnp.int32) * WINDOW,
-        own(sink_logit, 0),
-    )
-    attend_out = attended.reshape(length, heads * HEAD_DIM)
-    tokens = length // n
-
-    def by_side(flat):
-        split = flat.reshape(n, n_tp, tokens // n_tp, flat.shape[1])
-        return split.transpose(1, 0, 2, 3).reshape(n_tp, length // n_tp, flat.shape[1])
-
-    all_state, all_attend = join(n, by_side(state_out), by_side(attend_out))
+    by_side_state, by_side_attend = mixer(
+        gathered, norm_gain[None], w_ssm, w_query, w_kv, shift_cols, decay_rate, rotation,
+        input_parts, output_parts, skip_scale, sink_logit,
+    )
+    all_state, all_attend = join(n, by_side_state, by_side_attend)
     result = jnp.dot(all_state, ows, preferred_element_type=jnp.float32)
     result = result + jnp.dot(all_attend, owa, preferred_element_type=jnp.float32)
     return settle(n, result.astype(jnp.bfloat16))
@@ -626,7 +753,7 @@
         and 2 * HEAD_DIM == in_ssm.shape[1] // n
         and decay_rate.shape[0] % (8 * n) == 0
         and decay_rate.shape[0] * GROUP_CH == in_ssm.shape[1]
-        and inputs.shape[0] % 128 == 0
+        and inputs.shape[0] == BLOCK == WINDOW
         and inputs.shape[1] % 128 == 0
         and in_ssm.shape[0] % (16 * n_fs) == 0
         and args[13].shape[1] % 128 == 0

time: 132 us -> 97.1 us (0.74)
  matrix products: 34.3 us -> 2.67 us
  Pallas kernels: 75.1 us -> 86.3 us
  local copies, waits for them, and re-layouts: 14.4 us -> 6.79 us
  other arithmetic: 7.03 us -> 0.86 us
    dot_general x26 -> x0, matrix products: 31.6 us -> none  [the longest x4 11.3 us: recurrence(): jnp.dot(lift_im.reshape(groups * state_dim, BLOCK), triangle, precision=h...]
    pallas_call x0 -> x1, Pallas kernels: none -> 14.9 us  [mixer(): pl.pallas_call(entry, out_shape=[jax.ShapeDtypeStruct((2, length // 2, w_...]
    slice x20 -> x0, local copies, waits for them, and re-layouts: 5.46 us -> none  [the longest x9 2.84 us: windows(): return jnp.concatenate([split[:-1], split[1:]], axis=1)]
    pallas_call x1, Pallas kernels: 25 us -> 20.8 us  [join(): pl.pallas_call(functools.partial(join_kernel, n), out_shape=[jax.ShapeDty...]
    reduce_sum x2 -> x0, other arithmetic: 3.35 us -> none  [the longest x1 2.22 us: fast_body(): jnp.mean(widened * widened, axis=1, keepdims=True) + epsilon]
    another operation x2 -> x0, local copies, waits for them, and re-layouts: 1.88 us -> none  [the longest x1 1.04 us: by_side(): split = flat.reshape(n, n_tp, tokens // n_tp, flat.shape[1])]
    unnamed x27 -> x13, local copies, waits for them, and re-layouts: 4.88 us -> 6.45 us
    transpose x2 -> x0, local copies, waits for them, and re-layouts: 1.47 us -> none  [by_side(): split.transpose(1, 0, 2, 3).reshape(n_tp, length // n_tp, flat.shape[1])]
where the time goes in v2:
time: 97.1 us; the launch traced here: 96.7 us
  Pallas kernels  86.3 us (89%)
  local copies, waits for them, and re-layouts  6.79 us (7%)
  matrix products  2.67 us (3%)
    pallas_call x1, Pallas kernels, spread(): pl.pallas_call(functools.partial(spread_kernel, n, n_fs, n_tp, repeat_dev...  36.7 us
    pallas_call x1, Pallas kernels, join(): pl.pallas_call(functools.partial(join_kernel, n), out_shape=[jax.ShapeDty...  20.8 us
    pallas_call x1, Pallas kernels, mixer(): pl.pallas_call(entry, out_shape=[jax.ShapeDtypeStruct((2, length // 2, w_...  14.9 us
    pallas_call x1, Pallas kernels, settle(): pl.pallas_call(functools.partial(settle_kernel, n), out_shape=jax.ShapeDt...  13.8 us
    unnamed x13, local copies, waits for them, and re-layouts  6.45 us

profile of v2, /device:TPU:0, one launch (start us, length us, event | category | flops | bytes accessed | tf_op | source)
XLA Modules:
  0.0 96.7 jit_solution(10393075866748564130)
XLA Ops:
  0.0 0.0 copy-start.3
  0.0 1.4 %copy.23.refs_10_ = f32[32,16]{1,0:T(8,128)} copy(f32[32,16]{0,1:T(8,128)} %param.25) | data formatting | bytes 4096 | tf_op args[10]
  1.4 1.0 %copy.18 = bf16[512,128]{0,1:T(8,128)(2,1)S(1)} copy(bf16[512,128]{1,0:T(8,128)(2,1)} %param.19) | data formatting | bytes 262144 | tf_op args[4]
  2.4 0.2 copy.20
  2.6 1.0 %copy.19 = bf16[512,128]{0,1:T(8,128)(2,1)S(1)} copy(bf16[512,128]{1,0:T(8,128)(2,1)} %param.20) | data formatting | bytes 262144 | tf_op args[5]
  3.6 0.2 copy.21
  3.8 0.9 maximum_bitcast_fusion.kv
  4.6 0.0 copy-done.3
  4.6 1.3 %copy.22.refs_8_ = bf16[2,32,64,16]{3,2,1,0:T(8,128)(2,1)} copy(bf16[2,32,64,16]{2,3,1,0:T(8,128)(2,1)S(1)} %copy-done.3) | data formatting | bytes 262144 | tf_op args[8]
  6.0 36.7 %shard_map.145 = (bf16[512,2048]{1,0:T(8,128)(2,1)}, bf16[2048,128]{1,0:T(8,128)(2,1)}, bf16[2048,128]{1,0:T(8,128)(2,1)}, bf16[2048,128]{1,0:T(8,128)(2,1)}, f3...) custom-call(bf16[128,1024]{1,0:T(8,128)(2,1)} %x.1, bf16[512,512]{1,0:T(8,128)(2,1)} %ssm.1, ...), custom_call_target="tpu_custom_call" | custom-call | tf_op jit(solution)/shard_map/pallas_call | solution.py:436
  42.7 0.0 copy-start.1
  42.7 14.9 %shard_map.146 = (bf16[2,256,128]{2,1,0:T(8,128)(2,1)}, bf16[2,256,128]{2,1,0:T(8,128)(2,1)}) custom-call(bf16[512,2048]{1,0:T(8,128)(2,1)} %get-tuple-element.16.refs_0_, f32[1,2048]{1,0:T(1,128)} %bitcast.13, bf16[2048,128]{1,0:T(8,128)(2,1)} %get-tuple-element.17.refs_2_, bf16[2048,128]{1,0:T(8,128)(2,1)} %get-tuple-element.18.refs_3_, ...), custom_call_target="tpu_custom_call" | custom-call | tf_op jit(solution)/shard_map/pallas_call | solution.py:698
  57.7 0.0 copy-start
  57.7 20.8 %shard_map.147 = (bf16[256,1024]{1,0:T(8,128)(2,1)}, bf16[256,1024]{1,0:T(8,128)(2,1)}) custom-call(bf16[2,256,128]{2,1,0:T(8,128)(2,1)} %get-tuple-element.21.hs, bf16[2,256,128]{2,1,0:T(8,128)(2,1)} %get-tuple-element.22.ha), custom_call_target="tpu_custom_call" | custom-call | tf_op jit(solution)/shard_map/pallas_call | solution.py:494
  78.5 0.0 copy-start.2
  78.5 0.0 copy-done.1
  78.5 1.5 %fusion.1 = f32[256,512]{1,0:T(8,128)S(1)} fusion(bf16[256,1024]{1,0:T(8,128)(2,1)} %get-tuple-element.23, bf16[1024,512]{1,0:T(8,128)(2,1)S(1)} %copy-done.1), kind=kOutput, calls=%fused_computation.3 | convolution fusion | flops 268435456 | bytes 2097152 | tf_op jit(solution)/shard_map/dot_general | solution.py:735
  80.1 0.0 copy-done
  80.1 0.0 copy-done.2
  80.1 1.1 %fusion.src = bf16[256,512]{1,0:T(8,128)(2,1)} fusion(f32[256,512]{1,0:T(8,128)S(1)} %fusion.1, bf16[256,1024]{1,0:T(8,128)(2,1)S(1)} %copy-done.2, bf16[1024,512]{1,0:T(8,128)(2,1)S(1)} %copy-done), kind=kOutput, calls=%fused_computation.1 | convolution fusion | flops 268697600 | bytes 2359296 | tf_op jit(solution)/shard_map/dot_general | solution.py:736
  81.2 13.8 %shard_map.148 = bf16[64,2048]{1,0:T(8,128)(2,1)} custom-call(bf16[256,512]{1,0:T(8,128)(2,1)} %fusion.src), custom_call_target="tpu_custom_call" | custom-call | tf_op jit(solution)/shard_map/pallas_call | solution.py:531
  95.0 1.7 %copy.25 = bf16[64,2048]{1,0:T(8,128)(2,1)} copy(bf16[64,2048]{1,0:T(8,128)(2,1)} %shard_map.148) | data formatting | bytes 524288
Async XLA Ops:
  0.0 4.6 %copy-start.3 = (bf16[2,32,64,16]{2,3,1,0:T(8,128)(2,1)S(1)}, bf16[2,32,64,16]{2,3,1,0:T(8,128)(2,1)}, u32[]{:S(2)}) copy-start(bf16[2,32,64,16]{2,3,1,0:T(8,128)(2,1)} %param.23) | copy-start | bytes 393220
  42.7 35.8 %copy-start.1 = (bf16[1024,512]{1,0:T(8,128)(2,1)S(1)}, bf16[1024,512]{1,0:T(8,128)(2,1)}, u32[]{:S(2)}) copy-start(bf16[1024,512]{1,0:T(8,128)(2,1)} %get-tuple-element.24) | copy-start | bytes 3145732
  57.7 22.4 %copy-start = (bf16[1024,512]{1,0:T(8,128)(2,1)S(1)}, bf16[1024,512]{1,0:T(8,128)(2,1)}, u32[]{:S(2)}) copy-start(bf16[1024,512]{1,0:T(8,128)(2,1)} %get-tuple-element.26) | copy-start | bytes 3145732
  78.5 1.6 %copy-start.2 = (bf16[256,1024]{1,0:T(8,128)(2,1)S(1)}, bf16[256,1024]{1,0:T(8,128)(2,1)}, u32[]{:S(2)}) copy-start(bf16[256,1024]{1,0:T(8,128)(2,1)} %get-tuple-element.25) | copy-start | bytes 1572868

commit v3 on v2

--- a/solution.py
+++ b/solution.py
@@ -461,81 +461,140 @@
     )(x, ssm, query, kv, shift, ows, owa)
 
 
-def join_kernel(n, hs, ha, gs, ga, held, send, recv, in_sem, out_sem):
+def finish_kernel(n, hs, ha, ows, owa, out, got, passing, mixed,
+                  h_send, h_recv, p_send, p_recv, own_send, own_recv, o_send, o_recv, in_sem, out_sem):
     k = lax.axis_index("sp")
     t = lax.axis_index("tp")
-    width = hs.shape[2]
-    pairs = [(s, r) for s in range(n) for r in range(2) if (s, r) != (0, 0)]
-    pairs = sorted(pairs, key=lambda p: -min(p[0], n - p[0]))
-    greet([{"sp": lax.rem(k + s, n), "tp": lax.rem(t + r, 2)} for s, r in pairs])
-    columns = pl.ds(pl.multiple_of((t * n + k) * width, 128), width)
-    copies = []
-    for s, r in pairs:
-        for i, (src, dst) in enumerate(((hs, gs), (ha, ga))):
-            side = lax.rem(t + r, 2)
-            c = remote(src.at[side], dst.at[:, columns], send.at[i, s, r], recv.at[i, s, r],
-                       sp=lax.rem(k + s, n), tp=side)
-            c.start()
-            copies.append(c)
-    for i, (src, dst) in enumerate(((hs, gs), (ha, ga))):
-        c = pltpu.make_async_copy(src.at[t], held.at[i], in_sem.at[i])
+    other = 1 - t
+    sources = (hs, ha)
+    chunks = [(i, r) for r in (1, 0) for i in range(2)]
+    greet([{"sp": lax.rem(k + s, n)} for s in range(1, n)] + [{"tp": other}])
+
+    def landing(j, i, r):
+        return passing.at[i, j] if r else got.at[i, t * n + j]
+
+    def hop(step, way, chunk):
+        i, r = chunks[chunk]
+        origin = k - way * step
+        dst = landing(lax.rem(origin + n, n), i, r)
+        src = dst
+        if step == 0:
+            src = sources[i].at[other if r else t]
+        active = jnp.logical_and(k + way >= 0, k + way < n)
+        active = jnp.logical_and(active, jnp.logical_and(origin >= 0, origin < n))
+        w = 0 if way > 0 else 1
+        return active, remote(src, dst, h_send.at[w, step, chunk], h_recv.at[w, step, chunk],
+                              sp=lax.rem(k + way + n, n))
+
+    def arrival(step, way, chunk):
+        i, r = chunks[chunk]
+        origin = k - way * (step + 1)
+        active = jnp.logical_and(origin >= 0, origin < n)
+        j = lax.rem(origin + n, n)
+        w = 0 if way > 0 else 1
+        block = landing(j, i, r)
+        c = remote(block, block, h_send.at[w, step, chunk], h_recv.at[w, step, chunk],
+                   sp=lax.rem(k - way + n, n))
+        p = None
+        if r:
+            p = remote(block, got.at[i, t * n + j], p_send.at[w, step, i], p_recv.at[w, step, i],
+                       tp=other)
+        return active, c, p
+
+    for chunk in range(4):
+        for way in (1, -1):
+            active, c = hop(0, way, chunk)
+
+            @pl.when(active)
+            def _():
+                c.start()
+
+    own = []
+    for i in range(2):
+        c = remote(sources[i].at[other], got.at[i, t * n + k], own_send.at[i], own_recv.at[i], tp=other)
         c.start()
+        own.append(c)
+        c = pltpu.make_async_copy(sources[i].at[t], got.at[i, t * n + k], in_sem.at[i])
+        c.start()
+        own.append(c)
+    for step in range(n - 1):
+        for chunk in range(4):
+            for way in (1, -1):
+                active, c, p = arrival(step, way, chunk)
+
+                @pl.when(active)
+                def _():
+                    c.wait_recv()
+                    if p is not None:
+                        p.start()
+
+                if step + 1 < n - 1:
+                    further, onward = hop(step + 1, way, chunk)
+
+                    @pl.when(further)
+                    def _():
+                        onward.start()
+
+    for step in range(n - 1):
+        for chunk in range(4):
+            for way in (1, -1):
+                active, c = hop(step, way, chunk)
+
+                @pl.when(active)
+                def _():
+                    c.wait_send()
+
+                arrived, _c, p = arrival(step, way, chunk)
+                if p is not None:
+
+                    @pl.when(arrived)
+                    def _():
+                        p.wait()
+
+    for c in own:
         c.wait()
-        c = pltpu.make_async_copy(held.at[i], dst.at[:, columns], out_sem.at[i])
-        c.start()
-        c.wait()
-    for c in copies:
-        c.wait()
-
-
-def join(n, hs, ha):
-    _, rows, width = hs.shape
-    dma = pltpu.SemaphoreType.DMA
-    return pl.pallas_call(
-        functools.partial(join_kernel, n),
-        out_shape=[jax.ShapeDtypeStruct((rows, 2 * n * width), jnp.bfloat16)] * 2,
-        in_specs=[ANY] * 2,
-        out_specs=[ANY] * 2,
-        scratch_shapes=[pltpu.VMEM((2, rows, width), jnp.bfloat16),
-                        dma((2, n, 2)), dma((2, n, 2)), dma((2,)), dma((2,))],
-        compiler_params=pltpu.CompilerParams(collective_id=1, has_side_effects=True),
-    )(hs, ha)
-
-
-def settle_kernel(n, src, out, held, send, recv, in_sem, out_sem):
-    k = lax.axis_index("sp")
-    rows, width = src.shape[0] // n, src.shape[1]
-    order = sorted(range(1, n), key=lambda s: -min(s, n - s))
-    greet([{"sp": lax.rem(k + s, n)} for s in order])
+    total = None
+    for i, weights in enumerate((ows, owa)):
+        rows = jnp.concatenate([got[i, j] for j in range(2 * n)], axis=1)
+        term = jnp.dot(rows, weights[...], preferred_element_type=jnp.float32)
+        total = term if total is None else total + term
+    count, width = mixed.shape[1], mixed.shape[2]
+    for j in range(n):
+        mixed[j] = total[j * count : (j + 1) * count].astype(mixed.dtype)
     columns = pl.ds(pl.multiple_of(k * width, 128), width)
     copies = []
-    for s in order:
+    for s in sorted(range(1, n), key=lambda s: -min(s, n - s)):
         peer = lax.rem(k + s, n)
-        c = remote(src.at[pl.ds(pl.multiple_of(peer * rows, 16), rows)], out.at[:, columns],
-                   send.at[s], recv.at[s], sp=peer)
+        c = remote(mixed.at[peer], out.at[:, columns], o_send.at[s], o_recv.at[s], sp=peer)
         c.start()
         copies.append(c)
-    c = pltpu.make_async_copy(src.at[pl.ds(pl.multiple_of(k * rows, 16), rows)], held, in_sem.at[0])
-    c.start()
-    c.wait()
-    c = pltpu.make_async_copy(held, out.at[:, columns], out_sem.at[0])
+    c = pltpu.make_async_copy(mixed.at[k], out.at[:, columns], out_sem.at[0])
     c.start()
     c.wait()
     for c in copies:
         c.wait()
 
 
-def settle(n, mixed):
-    rows, width = mixed.shape[0] // n, mixed.shape[1]
+def finish(n, hs, ha, ows, owa):
+    _, rows, width = hs.shape
+    cols = ows.shape[1]
     dma = pltpu.SemaphoreType.DMA
+    vmem = pl.BlockSpec(memory_space=pltpu.VMEM)
+    bf = jnp.bfloat16
     return pl.pallas_call(
-        functools.partial(settle_kernel, n),
-        out_shape=jax.ShapeDtypeStruct((rows, n * width), jnp.bfloat16),
-        in_specs=[ANY],
+        functools.partial(finish_kernel, n),
+        out_shape=jax.ShapeDtypeStruct((rows // n, n * cols), bf),
+        in_specs=[vmem] * 4,
         out_specs=ANY,
-        scratch_shapes=[pltpu.VMEM((rows, width), jnp.bfloat16), dma((n,)), dma((n,)), dma((1,)), dma((1,))],
-        compiler_params=pltpu.CompilerParams(collective_id=2, has_side_effects=True),
-    )(mixed)
+        scratch_shapes=[
+            pltpu.VMEM((2, 2 * n, rows, width), bf),
+            pltpu.VMEM((2, n, rows, width), bf),
+            pltpu.VMEM((n, rows // n, cols), bf),
+            dma((2, n - 1, 4)), dma((2, n - 1, 4)), dma((2, n - 1, 2)), dma((2, n - 1, 2)),
+            dma((2,)), dma((2,)), dma((n,)), dma((n,)), dma((2,)), dma((1,)),
+        ],
+        compiler_params=pltpu.CompilerParams(collective_id=1, has_side_effects=True),
+    )(hs, ha, ows, owa)
 
 
 def halves(x):
@@ -610,20 +669,23 @@
         rise = jnp.exp(rates * away)
         up_re, up_im = rise * cos, -(rise * sin)
         down_re, down_im = fade * cos, fade * sin
-        damped = jnp.exp(-rates)
-        lift_re = damped * jnp.cos(turns) - 1.0
-        lift_im = damped * jnp.sin(turns)
-        modulus = rates * rates + turns * turns
-        factor_re = (turns * lift_im - rates * lift_re) / modulus
-        factor_im = -(turns * lift_re + rates * lift_im) / modulus
-        part_re = in_parts[0, first + g].astype(f32)
-        part_im = in_parts[1, first + g].astype(f32)
-        in_matrix = jnp.concatenate(
-            [factor_re * part_re - factor_im * part_im, factor_re * part_im + factor_im * part_re],
-            axis=0,
+        line, turn = rate[pl.ds(first + g, 1), :], rotation[pl.ds(first + g, 1), :]
+        damped = jnp.exp(-line)
+        lift_re = damped * jnp.cos(turn) - 1.0
+        lift_im = damped * jnp.sin(turn)
+        modulus = line * line + turn * turn
+        factor_re = (turn * lift_im - line * lift_re) / modulus
+        factor_im = -(turn * lift_re + line * lift_im) / modulus
+        part_re = in_parts[0, g].astype(f32)
+        part_im = in_parts[1, g].astype(f32)
+        in_matrix = jnp.transpose(
+            jnp.concatenate(
+                [factor_re * part_re - factor_im * part_im, factor_re * part_im + factor_im * part_re],
+                axis=1,
+            )
         ).astype(bf)
         read = jnp.concatenate(
-            [out_parts[0, first + g].astype(f32), -out_parts[1, first + g].astype(f32)], axis=1
+            [out_parts[0, g].astype(f32), -out_parts[1, g].astype(f32)], axis=1
         ).astype(bf)
         reach = jnp.exp(-rates * (centre + 1.0))
         reach_re = reach * jnp.cos(turns * (centre + 1.0))
@@ -639,7 +701,8 @@
         prefix = split_dot(jnp.concatenate(lifted, axis=0), tri)
         carry_re = jnp.zeros((state, 1), f32)
         carry_im = carry_re
-        skips = column(skip[pl.ds(first + g, 1), :])
+        chosen = lax.broadcasted_iota(jnp.int32, skip.shape, 1) == first + g
+        skips = jnp.sum(jnp.where(chosen, skip[...], 0.0), axis=1, keepdims=True)
         for b in range(blocks):
             span = slice(b * BLOCK, (b + 1) * BLOCK)
             begin = starts[b][g : g + 1, :]
@@ -719,22 +782,26 @@
 ):
     n, n_fs, n_tp = lax.axis_size("sp"), lax.axis_size("fs"), lax.axis_size("tp")
     key_heads = in_key.shape[1] // HEAD_DIM
-    rows = in_key.shape[0]
-    kv = jnp.concatenate(
-        [in_key.reshape(rows, key_heads, HEAD_DIM), in_value.reshape(rows, key_heads, HEAD_DIM)], axis=2
-    ).transpose(1, 0, 2)
+    kv = jnp.stack(
+        [
+            jnp.concatenate([array[:, h * HEAD_DIM : (h + 1) * HEAD_DIM] for array in (in_key, in_value)], axis=1)
+            for h in range(key_heads)
+        ]
+    )
     gathered, w_ssm, w_query, w_kv, shift_cols, ows, owa = spread(
         n, n_fs, n_tp, n // key_heads, inputs, in_ssm, in_query, kv,
         jnp.transpose(decay_shift), out_state, out_attend,
     )
+
+    def own(array):
+        size = array.shape[1] // n
+        return lax.dynamic_slice_in_dim(array, lax.axis_index("sp") * size, size, 1)
+
     by_side_state, by_side_attend = mixer(
         gathered, norm_gain[None], w_ssm, w_query, w_kv, shift_cols, decay_rate, rotation,
-        input_parts, output_parts, skip_scale, sink_logit,
-    )
-    all_state, all_attend = join(n, by_side_state, by_side_attend)
-    result = jnp.dot(all_state, ows, preferred_element_type=jnp.float32)
-    result = result + jnp.dot(all_attend, owa, preferred_element_type=jnp.float32)
-    return settle(n, result.astype(jnp.bfloat16))
+        own(jnp.swapaxes(input_parts, 2, 3)), own(output_parts), skip_scale.T, sink_logit,
+    )
+    return finish(n, by_side_state, by_side_attend, ows, owa)
 
 
 def body(*args):

time: 97.1 us -> 88.2 us (0.908)
  Pallas kernels: 86.3 us -> 80.1 us
  matrix products: 2.67 us -> 0 us
    pallas_call x2 -> x1, Pallas kernels: 34.6 us -> 29.4 us  [finish(): pl.pallas_call(functools.partial(finish_kernel, n), out_shape=jax.ShapeDt...]
    unnamed x13 -> x3, local copies, waits for them, and re-layouts: 6.45 us -> 2.62 us
    dot_general x2 -> x0, matrix products: 2.67 us -> none  [the longest x1 1.52 us: fast_body(): result = jnp.dot(all_state, ows, preferred_element_type=jnp.float32)]
    slice x0 -> x2, local copies, waits for them, and re-layouts: none -> 2.16 us  [fast_body(): array[:, h * HEAD_DIM:(h + 1) * HEAD_DIM]]
    dynamic_slice x0 -> x2, local copies, waits for them, and re-layouts: none -> 2.09 us  [own(): return lax.dynamic_slice_in_dim(array, lax.axis_index('sp') * size, size, 1)]
    pallas_call x1, Pallas kernels: 14.9 us -> 14 us  [mixer(): pl.pallas_call(entry, out_shape=[jax.ShapeDtypeStruct((2, length // 2, w_...]
where the time goes in v3:
time: 88.2 us; the launch traced here: 87.9 us
  Pallas kernels  80.1 us (91%)
  local copies, waits for them, and re-layouts  6.87 us (8%)
    pallas_call x1, Pallas kernels, spread(): pl.pallas_call(functools.partial(spread_kernel, n, n_fs, n_tp, repeat_dev...  36.7 us
    pallas_call x1, Pallas kernels, finish(): pl.pallas_call(functools.partial(finish_kernel, n), out_shape=jax.ShapeDt...  29.4 us
    pallas_call x1, Pallas kernels, mixer(): pl.pallas_call(entry, out_shape=[jax.ShapeDtypeStruct((2, length // 2, w_...  14 us
    unnamed x3, local copies, waits for them, and re-layouts  2.62 us
    slice x2, local copies, waits for them, and re-layouts, fast_body(): array[:, h * HEAD_DIM:(h + 1) * HEAD_DIM]  2.16 us
    dynamic_slice x2, local copies, waits for them, and re-layouts, own(): return lax.dynamic_slice_in_dim(array, lax.axis_index('sp') * size, size, 1)  2.09 us

profile of v3, /device:TPU:0, one launch (start us, length us, event | category | flops | bytes accessed | tf_op | source)
XLA Modules:
  0.0 87.9 jit_solution(15685853524621168928)
XLA Ops:
  0.0 0.0 copy-start
  0.0 0.9 %copy-done = bf16[2,32,64,16]{2,3,1,0:T(8,128)(2,1)S(1)} copy-done((bf16[2,32,64,16]{2,3,1,0:T(8,128)(2,1)S(1)}, bf16[2,32,64,16]{2,3,1,0:T(8,128)(2,1)}, u32[]{:S(2)}) %copy-start) | copy-done | bytes 131096
  1.0 0.6 dynamic-slice_bitcast_fusion.refs_8_
  1.6 1.5 %constant_dynamic-slice_fusion.refs_9_ = bf16[2,8,16,64]{3,2,1,0:T(8,128)(2,1)} fusion(bf16[2,32,16,64]{3,2,1,0:T(8,128)(2,1)} %param.24, s32[]{:T(128)S(6)} %select_n.4), kind=kLoop, calls=%fused_computation.4 | loop fusion | bytes 65540 | tf_op jit(solution)/shard_map/dynamic_slice | solution.py:798
  3.0 1.1 %fusion = (bf16[512,64]{1,0:T(8,128)(2,1)S(1)}, bf16[512,64]{1,0:T(8,128)(2,1)S(1)}) fusion(bf16[512,128]{1,0:T(8,128)(2,1)} %param.19), kind=kLoop, calls=%fused_computation.5 | loop fusion | bytes 262144 | tf_op jit(solution)/shard_map/slice | solution.py:787
  4.1 1.1 %fusion.1 = (bf16[512,64]{1,0:T(8,128)(2,1)S(1)}, bf16[512,64]{1,0:T(8,128)(2,1)S(1)}) fusion(bf16[512,128]{1,0:T(8,128)(2,1)} %param.20), kind=kLoop, calls=%fused_computation.6 | loop fusion | bytes 262144 | tf_op jit(solution)/shard_map/slice | solution.py:787
  5.2 0.1 maximum_bitcast_fusion
  5.4 0.7 pad_maximum_fusion.kv
  6.1 36.7 %shard_map.145 = (bf16[512,2048]{1,0:T(8,128)(2,1)}, bf16[2048,128]{1,0:T(8,128)(2,1)}, bf16[2048,128]{1,0:T(8,128)(2,1)}, bf16[2048,128]{1,0:T(8,128)(2,1)}, f3...) custom-call(bf16[128,1024]{1,0:T(8,128)(2,1)} %x.1, bf16[512,512]{1,0:T(8,128)(2,1)} %ssm.1, ...), custom_call_target="tpu_custom_call" | custom-call | tf_op jit(solution)/shard_map/pallas_call | solution.py:436
  42.8 14.0 %shard_map.146 = (bf16[2,256,128]{2,1,0:T(8,128)(2,1)}, bf16[2,256,128]{2,1,0:T(8,128)(2,1)}) custom-call(bf16[512,2048]{1,0:T(8,128)(2,1)} %get-tuple-element.14.refs_0_, f32[1,2048]{1,0:T(1,128)} %bitcast.10, bf16[2048,128]{1,0:T(8,128)(2,1)} %get-tuple-element.15.refs_2_, bf16[2048,128]{1,0:T(8,128)(2,1)} %get-tuple-element.16.refs_3_, ...), custom_call_target="tpu_custom_call" | custom-call | tf_op jit(solution)/shard_map/pallas_call | solution.py:761
  56.8 29.4 %shard_map.147 = bf16[64,2048]{1,0:T(8,128)(2,1)} custom-call(bf16[2,256,128]{2,1,0:T(8,128)(2,1)} %get-tuple-element.19.hs, bf16[2,256,128]{2,1,0:T(8,128)(2,1)} %get-tuple-element.20.ha, bf16[1024,512]{1,0:T(8,128)(2,1)} %get-tuple-element.21.ows, bf16[1024,512]{1,0:T(8,128)(2,1)} %get-tuple-element.22.owa), custom_call_target="tpu_custom_call" | custom-call | tf_op jit(solution)/shard_map/pallas_call | solution.py:584
  86.2 1.7 %copy.17 = bf16[64,2048]{1,0:T(8,128)(2,1)} copy(bf16[64,2048]{1,0:T(8,128)(2,1)} %shard_map.147) | data formatting | bytes 524288
Async XLA Ops:
  0.0 1.0 %copy-start = (bf16[2,32,64,16]{2,3,1,0:T(8,128)(2,1)S(1)}, bf16[2,32,64,16]{2,3,1,0:T(8,128)(2,1)}, u32[]{:S(2)}) copy-start(bf16[2,32,64,16]{2,3,1,0:T(8,128)(2,1)} %param.23) | copy-start | bytes 393220

commit v4 on v3

--- a/solution.py
+++ b/solution.py
@@ -685,7 +685,7 @@
             )
         ).astype(bf)
         read = jnp.concatenate(
-            [out_parts[0, g].astype(f32), -out_parts[1, g].astype(f32)], axis=1
+            [out_parts[0, first + g].astype(f32), -out_parts[1, first + g].astype(f32)], axis=1
         ).astype(bf)
         reach = jnp.exp(-rates * (centre + 1.0))
         reach_re = reach * jnp.cos(turns * (centre + 1.0))
@@ -799,7 +799,7 @@
 
     by_side_state, by_side_attend = mixer(
         gathered, norm_gain[None], w_ssm, w_query, w_kv, shift_cols, decay_rate, rotation,
-        own(jnp.swapaxes(input_parts, 2, 3)), own(output_parts), skip_scale.T, sink_logit,
+        own(jnp.swapaxes(input_parts, 2, 3)), output_parts, skip_scale.T, sink_logit,
     )
     return finish(n, by_side_state, by_side_attend, ows, owa)
 

time: 88.2 us -> 86.8 us (0.984)
  local copies, waits for them, and re-layouts: 6.87 us -> 5.4 us
    dynamic_slice x2 -> x1, local copies, waits for them, and re-layouts: 2.09 us -> 0.62 us  [own(): return lax.dynamic_slice_in_dim(array, lax.axis_index('sp') * size, size, 1)]
where the time goes in v4:
time: 86.8 us; the launch traced here: 86.5 us
  Pallas kernels  80.2 us (92%)
  local copies, waits for them, and re-layouts  5.4 us (6%)
  other arithmetic  0.88 us (1%)
    pallas_call x1, Pallas kernels, spread(): pl.pallas_call(functools.partial(spread_kernel, n, n_fs, n_tp, repeat_dev...  36.7 us
    pallas_call x1, Pallas kernels, finish(): pl.pallas_call(functools.partial(finish_kernel, n), out_shape=jax.ShapeDt...  29.4 us
    pallas_call x1, Pallas kernels, mixer(): pl.pallas_call(entry, out_shape=[jax.ShapeDtypeStruct((2, length // 2, w_...  14 us
    unnamed x3, local copies, waits for them, and re-layouts  2.62 us
    slice x2, local copies, waits for them, and re-layouts, fast_body(): array[:, h * HEAD_DIM:(h + 1) * HEAD_DIM]  2.16 us

profile of v4, /device:TPU:0, one launch (start us, length us, event | category | flops | bytes accessed | tf_op | source)
XLA Modules:
  0.0 86.5 jit_solution(15790388501440956135)
XLA Ops:
  0.0 0.0 copy-start
  0.0 0.9 %copy-done = bf16[2,32,64,16]{2,3,1,0:T(8,128)(2,1)S(1)} copy-done((bf16[2,32,64,16]{2,3,1,0:T(8,128)(2,1)S(1)}, bf16[2,32,64,16]{2,3,1,0:T(8,128)(2,1)}, u32[]{:S(2)}) %copy-start) | copy-done | bytes 131096
  1.0 0.6 dynamic-slice_bitcast_fusion.refs_8_
  1.6 1.1 %fusion = (bf16[512,64]{1,0:T(8,128)(2,1)S(1)}, bf16[512,64]{1,0:T(8,128)(2,1)S(1)}) fusion(bf16[512,128]{1,0:T(8,128)(2,1)} %param.19), kind=kLoop, calls=%fused_computation.4 | loop fusion | bytes 262144 | tf_op jit(solution)/shard_map/slice | solution.py:787
  2.7 1.1 %fusion.1 = (bf16[512,64]{1,0:T(8,128)(2,1)S(1)}, bf16[512,64]{1,0:T(8,128)(2,1)S(1)}) fusion(bf16[512,128]{1,0:T(8,128)(2,1)} %param.20), kind=kLoop, calls=%fused_computation.5 | loop fusion | bytes 262144 | tf_op jit(solution)/shard_map/slice | solution.py:787
  3.7 0.1 maximum_bitcast_fusion
  3.9 0.7 pad_maximum_fusion.kv
  4.6 36.7 %shard_map.145 = (bf16[512,2048]{1,0:T(8,128)(2,1)}, bf16[2048,128]{1,0:T(8,128)(2,1)}, bf16[2048,128]{1,0:T(8,128)(2,1)}, bf16[2048,128]{1,0:T(8,128)(2,1)}, f3...) custom-call(bf16[128,1024]{1,0:T(8,128)(2,1)} %x.1, bf16[512,512]{1,0:T(8,128)(2,1)} %ssm.1, ...), custom_call_target="tpu_custom_call" | custom-call | tf_op jit(solution)/shard_map/pallas_call | solution.py:436
  41.4 14.0 %shard_map.146 = (bf16[2,256,128]{2,1,0:T(8,128)(2,1)}, bf16[2,256,128]{2,1,0:T(8,128)(2,1)}) custom-call(bf16[512,2048]{1,0:T(8,128)(2,1)} %get-tuple-element.14.refs_0_, f32[1,2048]{1,0:T(1,128)} %bitcast.10, bf16[2048,128]{1,0:T(8,128)(2,1)} %get-tuple-element.15.refs_2_, bf16[2048,128]{1,0:T(8,128)(2,1)} %get-tuple-element.16.refs_3_, ...), custom_call_target="tpu_custom_call" | custom-call | tf_op jit(solution)/shard_map/pallas_call | solution.py:761
  55.4 29.4 %shard_map.147 = bf16[64,2048]{1,0:T(8,128)(2,1)} custom-call(bf16[2,256,128]{2,1,0:T(8,128)(2,1)} %get-tuple-element.19.hs, bf16[2,256,128]{2,1,0:T(8,128)(2,1)} %get-tuple-element.20.ha, bf16[1024,512]{1,0:T(8,128)(2,1)} %get-tuple-element.21.ows, bf16[1024,512]{1,0:T(8,128)(2,1)} %get-tuple-element.22.owa), custom_call_target="tpu_custom_call" | custom-call | tf_op jit(solution)/shard_map/pallas_call | solution.py:584
  84.8 1.7 %copy.17 = bf16[64,2048]{1,0:T(8,128)(2,1)} copy(bf16[64,2048]{1,0:T(8,128)(2,1)} %shard_map.147) | data formatting | bytes 524288
Async XLA Ops:
  0.0 1.0 %copy-start = (bf16[2,32,64,16]{2,3,1,0:T(8,128)(2,1)S(1)}, bf16[2,32,64,16]{2,3,1,0:T(8,128)(2,1)}, u32[]{:S(2)}) copy-start(bf16[2,32,64,16]{2,3,1,0:T(8,128)(2,1)} %param.23) | copy-start | bytes 393220
